TPU v7x, 32 devices: a whole 2x2x4 slice. The times are simulated.
32 devices in a mesh: sp: 8 (over z, x), tp: 4 (over y, core).
Axes of the slice: x: 2, y: 2, z: 4, core: 2. Of those that a mesh axis runs over, the one named last changes fastest.
Arguments:
- residual: bfloat16 [2048, 2048], P(('sp', 'tp')), may hold values from -6 to 6
- query_wide: bfloat16 [2048, 512], P('sp', 'tp'), may hold values from -8 to 8
- key_wide: bfloat16 [2048, 512], P('sp', 'tp'), may hold values from -8 to 8
- value_wide: bfloat16 [2048, 512], P('sp', 'tp'), may hold values from -6 to 6
- query_narrow: bfloat16 [2048, 512], P('sp', 'tp'), may hold values from -8 to 8
- key_narrow: bfloat16 [2048, 512], P('sp', 'tp'), may hold values from -8 to 8
- value_narrow: bfloat16 [2048, 512], P('sp', 'tp'), may hold values from -6 to 6
- gate_wide: float32 [2048, 4], P('sp', 'tp'), may hold values from -2 to 20
- gate_narrow: float32 [2048, 8], P('sp', 'tp'), may hold values from -2 to 20
- out_wide: bfloat16 [512, 2048], replicated, may hold values from -0.1875 to 0.1875
- out_narrow: bfloat16 [512, 2048], replicated, may hold values from -0.1875 to 0.1875
- norm_gain: float32 [2048], replicated, may hold values from 0.1 to 1.9
- routing: int32 [2048, 2], P(('sp', 'tp')), may hold values from 0 to 7, as said below
- route_weight: float32 [2048, 2], P(('sp', 'tp')), may hold values from 0.3 to 1.5
- gate_weight: bfloat16 [8, 2048, 1024], P('sp', None, 'tp'), may hold values from -0.125 to 0.125
- up_weight: bfloat16 [8, 2048, 1024], P('sp', None, 'tp'), may hold values from -0.125 to 0.125
- down_weight: bfloat16 [8, 1024, 2048], P('sp', 'tp'), may hold values from -0.1875 to 0.1875
Outputs:
- result: bfloat16 [2048, 2048], P(('sp', 'tp'))
Inputs may be any that keep to these rules, and one draw needn't show every extreme that they name: `routing`: each row names 2 different experts of one group (experts g * 2 to g * 2 + 1). In each aligned block of 64 rows (the rows of one device) no expert is named by more than 32 rows; one group, the same for all blocks, has each of its experts named by exactly 32 rows of every block.
All inputs are finite; a program needn't handle non-finite values.
Results may differ from a plain program's by a relative error of at most 0.017.
Values may be sent and summed in bfloat16 or wider, within the bound.
A program may use at most 128 MiB of HBM per device.

v0:
```python
import functools
import math

import jax
import jax.numpy as jnp
from jax import lax
from jax.experimental import pallas as pl
from jax.experimental.pallas import tpu as pltpu
from jax.sharding import PartitionSpec as P

HW = 128
HN = 64
GROUPS = 4


epsilon = 1e-06


def globalize(pieces, shard_rows):
    shards = pieces.shape[0] // shard_rows
    grid = pieces.reshape(shards, shard_rows, pieces.shape[1])
    endings = grid[:, -1, :]
    offsets = jnp.cumsum(endings, axis=0) - endings
    return (grid + offsets[:, None, :]).reshape(pieces.shape)


def head_block(
    state, queries, query_decay, keys, values, key_decay, first_key, first_query, head_width
):
    highest_old, weight_sum, weighted = state
    query_rows = queries.shape[0]
    head_count = query_decay.shape[1]
    key_rows = keys.shape[0]
    grid_query = queries.reshape(query_rows, head_count, head_width)
    grid_key = keys.reshape(key_rows, head_count, head_width)
    grid_value = values.reshape(key_rows, head_count, head_width)
    scores = jnp.einsum("thd,phd->htp", grid_query, grid_key, preferred_element_type=jnp.float32)
    scores = scores * head_width ** (-0.5) + query_decay.T[:, :, None] - key_decay.T[:, None, :]
    query_place = first_query + jnp.arange(query_rows, dtype=jnp.int32)
    key_place = first_key + jnp.arange(key_rows, dtype=jnp.int32)
    scores = jnp.where(key_place[None, None, :] <= query_place[None, :, None], scores, -jnp.inf)
    highest = jnp.maximum(highest_old, jnp.max(scores, axis=2))
    weights = jnp.exp(scores - highest[:, :, None])
    shrink = jnp.exp(highest_old - highest)
    weight_sum = weight_sum * shrink + jnp.sum(weights, axis=2)
    product = jnp.einsum(
        "htp,phd->htd", weights.astype(jnp.bfloat16), grid_value, preferred_element_type=jnp.float32
    )
    weighted = weighted * shrink[:, :, None] + product
    return (highest, weight_sum, weighted)


def fresh_state(head_count, shard_rows, head_width):
    return (
        jnp.full((head_count, shard_rows), -1e30, jnp.float32),
        jnp.zeros((head_count, shard_rows), jnp.float32),
        jnp.zeros((head_count, shard_rows, head_width), jnp.float32),
    )


def finish(state, shard_rows):
    highest, weight_sum, weighted = state
    mixed_heads = weighted / weight_sum[:, :, None]
    joined = jnp.transpose(mixed_heads, (1, 0, 2))
    return joined.reshape(shard_rows, weighted.shape[0] * weighted.shape[2]).astype(jnp.bfloat16)


def body(
    residual,
    query_wide,
    key_wide,
    value_wide,
    query_narrow,
    key_narrow,
    value_narrow,
    gate_wide,
    gate_narrow,
    out_wide,
    out_narrow,
    norm_gain,
    routing,
    route_weight,
    gate_weight,
    up_weight,
    down_weight,
):
    shard_rows = query_wide.shape[0]
    half_rows = shard_rows // 2
    sp_place = lax.axis_index("sp")
    first_query = sp_place * shard_rows
    running_wide = jnp.cumsum(jax.nn.log_sigmoid(gate_wide), axis=0)
    running_narrow = jnp.cumsum(jax.nn.log_sigmoid(gate_narrow), axis=0)
    pieces_wide, pieces_narrow = (
        lax.all_gather(running_wide, "sp", axis=0, tiled=True),
        lax.all_gather(running_narrow, "sp", axis=0, tiled=True),
    )
    every_wide = globalize(pieces_wide, shard_rows)
    every_narrow = globalize(pieces_narrow, shard_rows)
    late_first = first_query + half_rows
    halves = []
    for place, part_wide, part_narrow in (
        (first_query, query_wide[:half_rows], query_narrow[:half_rows]),
        (late_first, query_wide[half_rows:], query_narrow[half_rows:]),
    ):
        halves.append(
            (
                place,
                part_wide,
                part_narrow,
                lax.dynamic_slice_in_dim(every_wide, place, half_rows, 0),
                lax.dynamic_slice_in_dim(every_narrow, place, half_rows, 0),
            )
        )

    def half_state():
        return (
            fresh_state(gate_wide.shape[1], half_rows, HW),
            fresh_state(gate_narrow.shape[1], half_rows, HN),
        )

    state = (half_state(), half_state())
    keys_wide = lax.all_gather(key_wide, "sp", axis=0, tiled=True)
    values_wide = lax.all_gather(value_wide, "sp", axis=0, tiled=True)
    keys_narrow = lax.all_gather(key_narrow, "sp", axis=0, tiled=True)
    values_narrow = lax.all_gather(value_narrow, "sp", axis=0, tiled=True)
    span_rows = keys_wide.shape[0]
    block_size = math.gcd(span_rows, 2048)

    def visit(carried, position):
        inside = position * block_size

        def take_block(source):
            return lax.dynamic_slice_in_dim(source, inside, block_size, 0)

        def take_decay(source):
            return lax.dynamic_slice_in_dim(source, inside, block_size, 0)

        block_kw = take_block(keys_wide)
        block_vw = take_block(values_wide)
        block_kn = take_block(keys_narrow)
        block_vn = take_block(values_narrow)
        block_dw = take_decay(every_wide)
        block_dn = take_decay(every_narrow)

        def one_half(current, half):
            place, part_wide, part_narrow, query_decay_wide, query_decay_narrow = half

            def work(inner):
                first = head_block(
                    inner[0],
                    part_wide,
                    query_decay_wide,
                    block_kw,
                    block_vw,
                    block_dw,
                    inside,
                    place,
                    HW,
                )
                second = head_block(
                    inner[1],
                    part_narrow,
                    query_decay_narrow,
                    block_kn,
                    block_vn,
                    block_dn,
                    inside,
                    place,
                    HN,
                )
                return (first, second)

            def skip(inner):
                return inner

            return lax.cond(inside <= place + half_rows - 1, work, skip, current)

        updated = (one_half(carried[0], halves[0]), one_half(carried[1], halves[1]))
        return (updated, None)

    state, _ = lax.scan(visit, state, jnp.arange(span_rows // block_size, dtype=jnp.int32))
    att_wide = jnp.concatenate(
        [finish(state[0][0], half_rows), finish(state[1][0], half_rows)], axis=0
    )
    att_narrow = jnp.concatenate(
        [finish(state[0][1], half_rows), finish(state[1][1], half_rows)], axis=0
    )
    own_rows = residual.shape[0]
    tp_place = lax.axis_index("tp")
    rows_wide = lax.dynamic_slice_in_dim(
        out_wide, tp_place * att_wide.shape[1], att_wide.shape[1], 0
    )
    rows_narrow = lax.dynamic_slice_in_dim(
        out_narrow, tp_place * att_narrow.shape[1], att_narrow.shape[1], 0
    )
    first = jnp.dot(att_wide, rows_wide, preferred_element_type=jnp.float32)
    second = jnp.dot(att_narrow, rows_narrow, preferred_element_type=jnp.float32)
    mixed = lax.psum_scatter(
        (first + second).astype(jnp.bfloat16), "tp", scatter_dimension=0, tiled=True
    ).astype(jnp.float32)
    middle = (residual.astype(jnp.float32) + mixed).astype(jnp.bfloat16)
    middle_wide = middle.astype(jnp.float32)
    spread = jnp.mean(middle_wide * middle_wide, axis=1, keepdims=True)
    normed = (middle_wide * lax.rsqrt(spread + epsilon) * norm_gain).astype(jnp.bfloat16)
    features = normed.shape[1]
    chosen_count = routing.shape[1]
    expert_count = gate_weight.shape[0] * lax.axis_size("sp")
    capacity = own_rows * GROUPS // expert_count
    flat_routes = routing.reshape(-1)
    matches = (flat_routes[:, None] == jnp.arange(expert_count, dtype=jnp.int32)[None, :]).astype(
        jnp.int32
    )
    ranking = jnp.sum((jnp.cumsum(matches, axis=0) - matches) * matches, axis=1)
    placing = flat_routes * capacity + ranking
    picker = (
        placing[None, :] == jnp.arange(expert_count * capacity, dtype=jnp.int32)[:, None]
    ).astype(jnp.bfloat16)
    picker = jnp.sum(picker.reshape(expert_count * capacity, own_rows, chosen_count), axis=2)
    outgoing = jnp.dot(picker, normed, preferred_element_type=jnp.float32).astype(jnp.bfloat16)
    outgoing = outgoing.reshape(expert_count, capacity, features)
    arrived = lax.all_to_all(outgoing, "sp", split_axis=0, concat_axis=0, tiled=True)
    pooled = lax.all_gather(arrived.reshape(-1, features), "tp", axis=0, tiled=True)
    gate_value = jnp.dot(pooled, gate_weight[0], preferred_element_type=jnp.float32)
    up_value = jnp.dot(pooled, up_weight[0], preferred_element_type=jnp.float32)
    hidden = (jax.nn.silu(gate_value) * up_value).astype(jnp.bfloat16)
    answers = lax.psum_scatter(
        jnp.dot(hidden, down_weight[0], preferred_element_type=jnp.float32).astype(jnp.bfloat16),
        "tp",
        scatter_dimension=0,
        tiled=True,
    )
    returned = lax.all_to_all(
        answers.reshape(expert_count, capacity, features),
        "sp",
        split_axis=0,
        concat_axis=0,
        tiled=True,
    )
    picked = jnp.take(returned.reshape(expert_count * capacity, features), placing, axis=0)
    picked = picked.reshape(own_rows, chosen_count, features).astype(jnp.float32)
    combined = jnp.sum(route_weight[:, :, None] * picked, axis=1)
    return (middle_wide + combined).astype(jnp.bfloat16)


CORES = 2
MESH = pl.DeviceIdType.MESH
VMEM = pl.BlockSpec(memory_space=pltpu.VMEM)


def greet(peers):
    barrier = pltpu.get_barrier_semaphore()
    for peer in peers:
        pl.semaphore_signal(barrier, inc=1, device_id=peer, device_id_type=MESH)
    pl.semaphore_wait(barrier, len(peers))


def remote(source, target, send, receive, peer):
    return pltpu.make_async_remote_copy(
        src_ref=source,
        dst_ref=target,
        send_sem=send,
        recv_sem=receive,
        device_id=peer,
        device_id_type=MESH,
    )


def call(kernel, number, outs, scratch, args):
    return pl.pallas_call(
        kernel,
        out_shape=outs,
        in_specs=[VMEM] * len(args),
        out_specs=[VMEM] * len(outs),
        scratch_shapes=scratch,
        compiler_params=pltpu.CompilerParams(collective_id=number, has_side_effects=True),
    )(*args)


DMA = pltpu.SemaphoreType.DMA


def keys_kernel(outer, inner, count, *refs):
    ins, outs = refs[:count], refs[count : 2 * count]
    local, send_up, take_up, send_in, take_in = refs[2 * count :]
    place = lax.axis_index("sp")
    o, i = place // inner, place % inner
    tp = lax.axis_index("tp")

    def at(o_, i_):
        return (o_ * inner + i_, tp)

    greet(
        [at((o + d) % outer, i) for d in range(1, outer)]
        + [at(o, (i + d) % inner) for d in range(1, inner)]
    )
    other = at((o + 1) % outer, i)

    def up(t, a):
        slot = (o - t) * inner + i
        source = ins[a] if t == 0 else outs[a].at[slot]
        return remote(source, outs[a].at[slot], send_up.at[t, a], take_up.at[t, a], at(o + 1, i))

    def across(t, d, a):
        slot = (o - t) * inner + i
        source = ins[a] if t == 0 else outs[a].at[slot]
        return remote(
            source,
            outs[a].at[slot],
            send_in.at[t, d - 1, a],
            take_in.at[t, d - 1, a],
            at(o, (i + d) % inner),
        )

    def landed(slot, a, semaphore):
        remote(outs[a].at[slot], outs[a].at[slot], semaphore, semaphore, other).wait_recv()

    for a in range(count):
        pltpu.make_async_copy(ins[a], outs[a].at[place], local.at[a]).start()
    for t in range(outer):

        @pl.when(o >= t)
        def _(t=t):
            for a in range(count):
                if t > 0:
                    landed((o - t) * inner + i, a, take_up.at[t - 1, a])
                if t < outer - 1:

                    @pl.when(o + 1 < outer)
                    def _(a=a):
                        up(t, a).start()

                for d in range(1, inner):
                    if t > 0:
                        across(t, d, a).start()
                    else:

                        @pl.when((i + d) % inner > i)
                        def _(a=a, d=d):
                            across(t, d, a).start()

    for t in range(outer):

        @pl.when(o >= t)
        def _(t=t):
            for a in range(count):
                for d in range(1, inner):
                    giver = (i - d + inner) % inner
                    slot = (o - t) * inner + giver
                    if t > 0:
                        landed(slot, a, take_in.at[t, d - 1, a])
                        across(t, d, a).wait_send()
                    else:

                        @pl.when(giver < i)
                        def _(a=a, d=d, slot=slot):
                            landed(slot, a, take_in.at[0, d - 1, a])

                        @pl.when((i + d) % inner > i)
                        def _(a=a, d=d):
                            across(0, d, a).wait_send()

                if t < outer - 1:

                    @pl.when(o + 1 < outer)
                    def _(a=a):
                        up(t, a).wait_send()

    for a in range(count):
        pltpu.make_async_copy(ins[a], outs[a].at[place], local.at[a]).wait()


def gather_keys(arrays, outer, inner):
    count = len(arrays)
    outs = [jax.ShapeDtypeStruct((outer * inner,) + x.shape, x.dtype) for x in arrays]
    scratch = [
        DMA((count,)),
        DMA((outer, count)),
        DMA((outer, count)),
        DMA((outer, inner, count)),
        DMA((outer, inner, count)),
    ]
    return call(functools.partial(keys_kernel, outer, inner, count), 1, outs, scratch, arrays)


def attend_kernel(qw, qn, near, kw, vw, kn, vn, far, out, top, total, mixed):
    place = lax.axis_index("sp")
    rows = qw.shape[0]
    width = qn.shape[1]
    heads = 1 + width // HN
    lanes = lax.broadcasted_iota(jnp.int32, (rows, width), 1) // HN

    def query(h):
        if h == 0:
            return qw[...]
        return jnp.where(lanes == h - 1, qn[...], jnp.zeros_like(qn[...]))

    def block(j, shift, diagonal):
        for h in range(heads):
            keys, values = (kw, vw) if h == 0 else (kn, vn)
            size = HW if h == 0 else HN
            scores = lax.dot_general(
                query(h), keys[j], (((1,), (1,)), ((), ())), preferred_element_type=jnp.float32
            )
            drop = (near[:, h : h + 1] + shift[h]) - far[j, h : h + 1, :]
            scores = scores * size ** (-0.5) + drop
            if diagonal:
                t = lax.broadcasted_iota(jnp.int32, scores.shape, 0)
                s = lax.broadcasted_iota(jnp.int32, scores.shape, 1)
                scores = jnp.where(s <= t, scores, -jnp.inf)
            peak = jnp.max(scores, axis=1, keepdims=True)
            if diagonal:
                weights = jnp.exp(scores - peak)
                total[h] = jnp.sum(weights, axis=1, keepdims=True)
                mixed[h] = jnp.dot(
                    weights.astype(jnp.bfloat16), values[j], preferred_element_type=jnp.float32
                )
                top[h] = peak
            else:
                before = top[h]
                peak = jnp.maximum(before, peak)
                weights = jnp.exp(scores - peak)
                shrink = jnp.exp(before - peak)
                total[h] = total[h] * shrink + jnp.sum(weights, axis=1, keepdims=True)
                mixed[h] = mixed[h] * shrink + jnp.dot(
                    weights.astype(jnp.bfloat16), values[j], preferred_element_type=jnp.float32
                )
                top[h] = peak

    block(place, [jnp.zeros((1, 1), jnp.float32)] * heads, True)

    def step(t, shift):
        j = place - 1 - t
        shift = tuple(shift[h] + far[j, h : h + 1, rows - 1 : rows] for h in range(heads))
        block(j, shift, False)
        return shift

    lax.fori_loop(0, place, step, tuple(jnp.zeros((1, 1), jnp.float32) for _ in range(heads)))
    out[:, : qw.shape[1]] = (mixed[0] / total[0]).astype(jnp.bfloat16)
    narrow = mixed[1] / total[1]
    for h in range(2, heads):
        narrow = jnp.where(lanes == h - 1, mixed[h] / total[h], narrow)
    out[:, qw.shape[1] :] = narrow.astype(jnp.bfloat16)


def swap_kernel(axis, n, stride, source, target, local, send, take):
    sp, tp = lax.axis_index("sp"), lax.axis_index("tp")
    me = (sp if axis == "sp" else tp) // stride
    rest = (sp if axis == "sp" else tp) % stride

    def at(k):
        return (k * stride + rest, tp) if axis == "sp" else (sp, k * stride + rest)

    greet([at((me + d) % n) for d in range(1, n)])

    def copy(d):
        k = (me + d) % n
        return remote(source.at[k], target.at[me], send.at[d], take.at[d], at(k))

    for d in range(1, n):
        copy(d).start()
    own = pltpu.make_async_copy(source.at[me], target.at[me], local.at[0])
    own.start()
    own.wait()
    for d in range(1, n):
        slot = target.at[(me - d + n) % n]
        remote(slot, slot, send.at[d], take.at[d], at((me + d) % n)).wait_recv()
        copy(d).wait_send()


def swap(array, axis, n, stride, number):
    return call(
        functools.partial(swap_kernel, axis, n, stride),
        number,
        [jax.ShapeDtypeStruct(array.shape, array.dtype)],
        [DMA((1,)), DMA((n,)), DMA((n,))],
        [array],
    )[0]


def spread_kernel(outer, inner, ys, count, *refs):
    ins, outs = refs[:count], refs[count : 2 * count]
    local, send_a, take_a, send_b, take_b, send_c, take_c = refs[2 * count :]
    place, tp = lax.axis_index("sp"), lax.axis_index("tp")
    o, i, y, c = place // inner, place % inner, tp // CORES, tp % CORES
    steps = [(di, dy) for di in range(inner) for dy in range(ys) if (di, dy) != (0, 0)]
    mate = (place, y * CORES + 1 - c)

    def beside(di, dy):
        return (o * inner + (i + di) % inner, (y + dy) % ys * CORES + c)

    def above(d):
        return ((o + d) % outer * inner + i, tp)

    greet(
        [above(d) for d in range(1, outer)] + [beside(di, dy) for di, dy in steps] + [mate]
    )

    def slot(a, core, t, di, dy):
        return outs[a].at[
            core, (o - t + outer) % outer, (i - di + inner) % inner, (y - dy + ys) % ys
        ]

    def first(d, a):
        return remote(
            ins[a].at[(o + d) % outer],
            outs[a].at[c, o, i, y],
            send_a.at[d, a],
            take_a.at[d, a],
            above(d),
        )

    def second(t, di, dy, a):
        source = ins[a].at[o] if t == 0 else slot(a, c, t, 0, 0)
        return remote(
            source,
            slot(a, c, t, 0, 0),
            send_b.at[t, di, dy, a],
            take_b.at[t, di, dy, a],
            beside(di, dy),
        )

    def third(t, di, dy, a):
        source = ins[a].at[o] if (t, di, dy) == (0, 0, 0) else slot(a, c, t, di, dy)
        return remote(
            source, slot(a, c, t, di, dy), send_c.at[t, di, dy, a], take_c.at[t, di, dy, a], mate
        )

    def landed(where, semaphore):
        remote(where, where, semaphore, semaphore, mate).wait_recv()

    def relay(t):
        for di, dy in steps:
            for a in range(count):
                landed(slot(a, c, t, di, dy), take_b.at[t, di, dy, a])
                third(t, di, dy, a).start()

    for d in range(1, outer):
        for a in range(count):
            first(d, a).start()
    for t in range(outer):
        for a in range(count):
            if t == 0:
                pltpu.make_async_copy(ins[a].at[o], slot(a, c, 0, 0, 0), local.at[a]).start()
            else:
                landed(slot(a, c, t, 0, 0), take_a.at[t, a])
            for di, dy in reversed(steps):
                second(t, di, dy, a).start()
            third(t, 0, 0, a).start()
        if t > 0:
            relay(t - 1)
    relay(outer - 1)
    for a in range(count):
        pltpu.make_async_copy(ins[a].at[o], slot(a, c, 0, 0, 0), local.at[a]).wait()
        for d in range(1, outer):
            first(d, a).wait_send()
        for t in range(outer):
            for di, dy in [(0, 0)] + steps:
                landed(slot(a, 1 - c, t, di, dy), take_c.at[t, di, dy, a])
                third(t, di, dy, a).wait_send()
                if (di, dy) != (0, 0):
                    second(t, di, dy, a).wait_send()


def spread_rows(arrays, outer, inner, ys):
    count = len(arrays)
    outs = [
        jax.ShapeDtypeStruct((CORES, outer, inner, ys) + x.shape[1:], x.dtype) for x in arrays
    ]
    wide = DMA((outer, inner, ys, count))
    scratch = [DMA((count,)), DMA((outer, count)), DMA((outer, count)), wide, wide, wide, wide]
    return call(
        functools.partial(spread_kernel, outer, inner, ys, count), 3, outs, scratch, arrays
    )


def mate_kernel(pieces, source, target, send, take):
    place, tp = lax.axis_index("sp"), lax.axis_index("tp")
    y, c = tp // CORES, tp % CORES
    mate = (place, y * CORES + 1 - c)
    greet([mate])

    def copy(p):
        return remote(source.at[1 - c, p], target.at[p], send.at[p], take.at[p], mate)

    for p in range(pieces):
        copy(p).start()
    for p in range(pieces):
        copy(p).wait()


def plane_kernel(outer, inner, ys, source, target, send, take):
    place, tp = lax.axis_index("sp"), lax.axis_index("tp")
    o, i, y, c = place // inner, place % inner, tp // CORES, tp % CORES
    steps = [(di, dy) for di in range(inner) for dy in range(ys) if (di, dy) != (0, 0)]

    def beside(di, dy):
        return (o * inner + (i + di) % inner, (y + dy) % ys * CORES + c)

    greet([beside(di, dy) for di, dy in steps])

    def copy(n, k):
        di, dy = steps[n]
        return remote(
            source.at[k, (i + di) % inner, (y + dy) % ys],
            target.at[n, k],
            send.at[n, k],
            take.at[n, k],
            beside(di, dy),
        )

    for k in range(outer):
        for n in reversed(range(len(steps))):
            copy(n, k).start()
    for k in range(outer):
        for n in range(len(steps)):
            copy(n, k).wait()


def fast_body(
    residual,
    query_wide,
    key_wide,
    value_wide,
    query_narrow,
    key_narrow,
    value_narrow,
    gate_wide,
    gate_narrow,
    out_wide,
    out_narrow,
    norm_gain,
    routing,
    route_weight,
    gate_weight,
    up_weight,
    down_weight,
):
    inner = routing.shape[1]
    places = lax.axis_size("sp")
    outer = places // inner
    parts = lax.axis_size("tp")
    ys = parts // CORES
    core = lax.axis_index("tp") % CORES
    y = lax.axis_index("tp") // CORES
    i = lax.axis_index("sp") % inner
    own_rows, features = residual.shape

    gates = jnp.concatenate([gate_wide, gate_narrow], axis=1).T
    running = jnp.cumsum(jax.nn.log_sigmoid(gates), axis=1)
    heads = gates.shape[0]
    far = jnp.pad(running, ((0, -heads % 8), (0, 0)))
    keys_wide, values_wide, keys_narrow, values_narrow, far = gather_keys(
        [key_wide, value_wide, key_narrow, value_narrow, far], outer, inner
    )
    shard_rows, wide = query_wide.shape
    narrow = query_narrow.shape[1]
    att = pl.pallas_call(
        attend_kernel,
        out_shape=jax.ShapeDtypeStruct((shard_rows, wide + narrow), jnp.bfloat16),
        in_specs=[VMEM] * 8,
        out_specs=VMEM,
        scratch_shapes=[
            pltpu.VMEM((heads, shard_rows, 1), jnp.float32),
            pltpu.VMEM((heads, shard_rows, 1), jnp.float32),
            pltpu.VMEM((heads, shard_rows, wide), jnp.float32),
        ],
    )(
        query_wide,
        query_narrow,
        running.T,
        keys_wide,
        values_wide,
        keys_narrow,
        values_narrow,
        far,
    )
    att = swap(att.reshape(parts, own_rows, wide + narrow), "tp", parts, 1, 2)
    att_wide = jnp.transpose(att[:, :, :wide], (1, 0, 2)).reshape(own_rows, parts * wide)
    att_narrow = jnp.transpose(att[:, :, wide:], (1, 0, 2)).reshape(own_rows, parts * narrow)
    mixed = jnp.dot(att_wide, out_wide, preferred_element_type=jnp.float32)
    mixed = mixed + jnp.dot(att_narrow, out_narrow, preferred_element_type=jnp.float32)
    middle = (residual.astype(jnp.float32) + mixed).astype(jnp.bfloat16)
    middle_wide = middle.astype(jnp.float32)
    spread = jnp.mean(middle_wide * middle_wide, axis=1, keepdims=True)
    normed = (middle_wide * lax.rsqrt(spread + epsilon) * norm_gain).astype(jnp.bfloat16)

    capacity = own_rows * GROUPS // places
    group = routing[:, 0] // inner
    matches = (group[:, None] == jnp.arange(GROUPS, dtype=jnp.int32)[None, :]).astype(jnp.int32)
    ranking = jnp.sum((jnp.cumsum(matches, axis=0) - matches) * matches, axis=1)
    placing = group * capacity + ranking
    picker = placing[None, :] == jnp.arange(GROUPS * capacity, dtype=jnp.int32)[:, None]
    of_expert = jnp.sum(
        jnp.where(
            (routing % inner)[:, :, None] == jnp.arange(inner, dtype=jnp.int32)[None, None, :],
            route_weight[:, :, None],
            0.0,
        ),
        axis=1,
    )
    slot_weight = jnp.sum(jnp.where(picker[:, :, None], of_expert[None, :, :], 0.0), axis=1)
    slot_weight = jnp.pad(slot_weight, ((0, 0), (0, -inner % 128)))
    picker = picker.astype(jnp.bfloat16)
    outgoing = jnp.dot(picker, normed, preferred_element_type=jnp.float32).astype(jnp.bfloat16)
    pooled, pooled_weight = spread_rows(
        [
            outgoing.reshape(GROUPS, capacity, features),
            slot_weight.reshape(GROUPS, capacity, slot_weight.shape[1]),
        ],
        outer,
        inner,
        ys,
    )
    pooled = pooled.reshape(-1, features)
    pooled_weight = pooled_weight.reshape(pooled.shape[0], -1)
    scale = jnp.where(i == 0, pooled_weight[:, :1], 0.0)
    for other in range(1, inner):
        scale = jnp.where(i == other, pooled_weight[:, other : other + 1], scale)
    gate_value = jnp.dot(pooled, gate_weight[0], preferred_element_type=jnp.float32)
    up_value = jnp.dot(pooled, up_weight[0], preferred_element_type=jnp.float32)
    hidden = (jax.nn.silu(gate_value) * up_value).astype(jnp.bfloat16)
    answers = jnp.dot(hidden, down_weight[0], preferred_element_type=jnp.float32)
    answers = (answers * scale).astype(jnp.bfloat16)
    answers = answers.reshape(CORES, outer, inner, ys, capacity, features)
    half = jax.ShapeDtypeStruct(answers.shape[1:], jnp.bfloat16)
    arrived = call(
        functools.partial(mate_kernel, outer),
        4,
        [half],
        [DMA((outer,)), DMA((outer,))],
        [answers],
    )[0]
    own = lax.dynamic_index_in_dim(answers, core, 0, keepdims=False)
    chip = (own.astype(jnp.float32) + arrived.astype(jnp.float32)).astype(jnp.bfloat16)
    others = inner * ys - 1
    arrived = call(
        functools.partial(plane_kernel, outer, inner, ys),
        5,
        [jax.ShapeDtypeStruct((others, outer, capacity, features), jnp.bfloat16)],
        [DMA((others, outer)), DMA((others, outer))],
        [chip],
    )[0]
    own = lax.dynamic_slice(
        chip, (0, i, y, 0, 0), (outer, 1, 1, capacity, features)
    ).reshape(outer, capacity, features)
    plane = own.astype(jnp.float32) + jnp.sum(arrived.astype(jnp.float32), axis=0)
    returned = swap(plane.astype(jnp.bfloat16), "sp", outer, inner, 6)
    combined = jnp.dot(
        picker.T, returned.reshape(-1, features), preferred_element_type=jnp.float32
    )
    return (middle_wide + combined).astype(jnp.bfloat16)


def choose(*args):
    routing, gate_weight = args[12], args[14]
    experts = gate_weight.shape[0] * lax.axis_size("sp")
    paired = lax.axis_size("tp") % CORES == 0 and gate_weight.shape[0] == 1
    if paired and experts == GROUPS * routing.shape[1]:
        return fast_body(*args)
    return body(*args)


def solution(mesh):
    placed = (
        P(("sp", "tp"), None),
        P("sp", "tp"),
        P("sp", "tp"),
        P("sp", "tp"),
        P("sp", "tp"),
        P("sp", "tp"),
        P("sp", "tp"),
        P("sp", "tp"),
        P("sp", "tp"),
        P(),
        P(),
        P(),
        P(("sp", "tp"), None),
        P(("sp", "tp"), None),
        P("sp", None, "tp"),
        P("sp", None, "tp"),
        P("sp", "tp", None),
    )
    return jax.shard_map(
        choose, mesh=mesh, in_specs=placed, out_specs=P(("sp", "tp"), None), check_vma=False
    )
```

profile of v0, /device:TPU:16, one launch (start us, length us, event | category | flops | bytes accessed | tf_op | source)
XLA Modules:
  0.0 179.9 jit_solution(697721297730779662)
XLA Ops:
  0.0 0.0 copy-start
  0.0 0.9 fusion.28
  0.9 0.9 reduce-window.6
  1.8 0.1 slice.28
  1.9 0.1 copy.40
  2.0 0.1 copy.41
  2.1 0.1 broadcast_add_fusion
  2.2 0.1 copy.42
  2.4 0.0 copy-start.2
  2.4 0.1 copy.55
  2.4 0.6 pad.8.clone.refs_4_
  3.1 22.9 %shard_map.163 = (bf16[8,256,128]{2,1,0:T(8,128)(2,1)}, bf16[8,256,128]{2,1,0:T(8,128)(2,1)}, bf16[8,256,128]{2,1,0:T(8,128)(2,1)}, bf16[8,256,128]{2,1,0:T(8,128)(2,1)}, f32[8,8,256]{2,1,0:T(8,128)}) custom-call(bf16[256,128]{1,0:T(8,128)(2,1)} %refs_0_.1, bf16[256,128]{1,0:T(8,128)(2,1)} %refs_1_.1, bf16[256,128]{1,0:T(8,128)(2,1)} %refs_2_.1, ...), custom_call_target="tpu_custom_call" | custom-call | tf_op jit(solution)/shard_map/pallas_call | solution.py:269
  26.0 0.0 copy-done.2
  26.0 11.1 %shard_map.164 = bf16[256,256]{1,0:T(8,128)(2,1)} custom-call(bf16[256,128]{1,0:T(8,128)(2,1)} %qw.1, bf16[256,128]{1,0:T(8,128)(2,1)} %qn.1, f32[256,3]{1,0:T(8,128)} %bitcast.71, bf16[8,256,128]{2,1,0:T(8,128)(2,1)} %get-tuple-element.12.kw, bf16[8,256,128]{2,1,0:T(8,128)(2,1)} %get-tuple-element.13.vw, bf16[8,256,128]{2,1,0:T(8,128)(2,1)} %get-tuple-element.14.kn, ...), custom_call_target="tpu_custom_call" | custom-call | tf_op jit(solution)/shard_map/pallas_call | solution.py:657
  37.0 5.7 %shard_map.165 = bf16[4,64,256]{2,1,0:T(8,128)(2,1)} custom-call(bf16[4,64,256]{2,1,0:T(8,128)(2,1)} %bitcast.72), custom_call_target="tpu_custom_call" | custom-call | tf_op jit(solution)/shard_map/pallas_call | solution.py:269
  42.8 0.9 slice_bitcast_fusion
  43.6 2.1 %fusion.22 = f32[64,2048]{1,0:T(8,128)S(1)} fusion(bf16[512,2048]{1,0:T(8,128)(2,1)} %param.26, bf16[4,8,8,128]{3,2,1,0:T(8,128)(2,1)S(1)} %get-tuple-element.22), kind=kOutput, calls=%fused_computation.32 | convolution fusion | flops 134217728 | bytes 2686976 | tf_op jit(solution)/shard_map/dot_general | solution.py:680
  45.7 0.0 copy-start.6
  45.7 0.0 copy-start.4
  45.8 0.0 copy-done
  45.8 0.0 copy-done.3
  45.8 0.0 copy-start.5
  45.8 0.6 multiply_reduce_fusion
  46.4 0.0 copy-done.6
  46.4 0.1 fusion.25
  46.5 0.1 reduce_window_sum.28
  46.6 0.2 select_reduce_fusion.1
  46.8 1.2 convolution_convert_fusion
  48.0 0.1 iota_compare_fusion
  48.1 0.0 copy-done.5
  48.2 0.1 select_reduce_fusion
  48.3 0.1 copy.56
  48.4 0.6 pad.9.clone
  49.0 47.4 %shard_map.166 = (bf16[2,4,2,2,32,2048]{5,4,3,2,1,0:T(8,128)(2,1)}, f32[2,4,2,2,32,128]{5,4,3,2,1,0:T(8,128)}) custom-call(bf16[4,32,2048]{2,1,0:T(8,128)(2,1)} %bitcast.67, f32[4,32,128]{2,1,0:T(8,128)} %bitcast.73), custom_call_target="tpu_custom_call" | custom-call | tf_op jit(solution)/shard_map/pallas_call | solution.py:269
  96.5 2.2 %fusion.34 = (f32[1024,1]{1,0:T(8,128)S(1)}, f32[1024,1]{1,0:T(8,128)}) fusion(f32[1024,128]{1,0:T(8,128)} %bitcast.69), kind=kLoop, calls=%fused_computation.71 | loop fusion | bytes 16384 | tf_op jit(solution)/shard_map/slice | solution.py:716
  98.7 1.2 copy.52
  99.9 0.2 copy.53
  100.1 4.8 %fusion.10 = f32[1024,256]{1,0:T(8,128)} fusion(bf16[1024,2048]{1,0:T(8,128)(2,1)} %bitcast.76, bf16[1,2048,256]{2,1,0:T(8,128)(2,1)} %param.31), kind=kOutput, calls=%fused_computation.18 | convolution fusion | flops 1073741824 | bytes 6291456 | tf_op jit(solution)/shard_map/dot_general | solution.py:719
  104.9 9.4 %multiply_convert_fusion = bf16[1024,2048]{1,0:T(8,128)(2,1)} fusion(f32[1024]{0:T(1024)S(1)} %bitcast.74, bf16[1024,2048]{1,0:T(8,128)(2,1)} %bitcast.77, bf16[1,256,2048]{2,1,0:T(8,128)(2,1)} %param.33, bf16[1,2048,256]{2,1,0:T(8,128)(2,1)} %param.32, f32[1024,256]{1,0:T(8,128)} %fusion.10), kind=kOutput, calls=%fused_computation | convolution fusion | flops 2153250816 | bytes 11538432 | tf_op jit(solution)/shard_map/dot_general | solution.py:722
  114.3 7.8 %shard_map.167 = bf16[4,2,2,32,2048]{4,3,2,1,0:T(8,128)(2,1)} custom-call(bf16[2,4,2,2,32,2048]{5,4,3,2,1,0:T(8,128)(2,1)} %bitcast.65), custom_call_target="tpu_custom_call" | custom-call | tf_op jit(solution)/shard_map/pallas_call | solution.py:269
  122.1 3.0 %fusion = bf16[4,2,2,32,2048]{4,3,0,2,1:T(8,128)(2,1)S(1)} fusion(bf16[4,2,2,32,2048]{4,3,2,1,0:T(8,128)(2,1)} %shard_map.167, bf16[2,4,2,2,32,2048]{5,4,3,2,1,0:T(8,128)(2,1)} %bitcast.66, s32[]{:T(128)S(6)} %select_n.84), kind=kLoop, calls=%fused_computation.2 | loop fusion | flops 4194304 | bytes 6291460 | tf_op jit(solution)/shard_map/convert_element_type | solution.py:734
  125.2 1.3 copy-done.1
  126.5 1.4 copy.51.source
  127.9 29.0 %shard_map.168 = bf16[3,4,32,2048]{3,2,1,0:T(8,128)(2,1)} custom-call(bf16[4,2,2,32,2048]{4,3,2,1,0:T(8,128)(2,1)} %copy.51.source), custom_call_target="tpu_custom_call" | custom-call | tf_op jit(solution)/shard_map/pallas_call | solution.py:269
  157.0 2.8 %convert_reduce_fusion = f32[4,32,2048]{2,1,0:T(8,128)} fusion(bf16[3,4,32,2048]{3,2,1,0:T(8,128)(2,1)} %shard_map.168), kind=kLoop, calls=%fused_computation.3 | loop fusion | flops 1310720 | bytes 2621440 | tf_op jit(solution)/shard_map/reduce_sum | solution.py:746
  159.7 2.3 %fusion.6.source = bf16[4,32,2048]{2,1,0:T(8,128)(2,1)} fusion(f32[4,32,2048]{2,1,0:T(8,128)} %convert_reduce_fusion, bf16[4,2,2,32,2048]{4,3,0,2,1:T(8,128)(2,1)} %copy-done.1, s32[]{:T(128)S(6)} %select_n.85, s32[]{:T(128)S(6)} %select_n.87), kind=kLoop, calls=%fused_computation.15 | loop fusion | flops 786432 | bytes 2097160 | tf_op jit(solution)/shard_map/convert_element_type | solution.py:747
  162.0 15.9 %shard_map.169 = bf16[4,32,2048]{2,1,0:T(8,128)(2,1)} custom-call(bf16[4,32,2048]{2,1,0:T(8,128)(2,1)} %fusion.6.source), custom_call_target="tpu_custom_call" | custom-call | tf_op jit(solution)/shard_map/pallas_call | solution.py:269
  177.9 2.0 %fusion.4 = bf16[64,2048]{1,0:T(8,128)(2,1)} fusion(f32[64,2048]{1,0:T(8,128)S(1)} %get-tuple-element.24, bf16[128,2048]{1,0:T(8,128)(2,1)} %bitcast.68, s32[64]{0:T(128)S(1)} %multiply_add_fusion), kind=kOutput, calls=%fused_computation.10 | convolution fusion | flops 33824768 | bytes 1310976 | tf_op jit(solution)/shard_map/dot_general | solution.py:748
  (12 shorter events, 0.1 us)
Async XLA Ops:
  0.0 45.8 %copy-start = (bf16[512,2048]{1,0:T(8,128)(2,1)S(1)}, bf16[512,2048]{1,0:T(8,128)(2,1)}, u32[]{:S(2)}) copy-start(bf16[512,2048]{1,0:T(8,128)(2,1)} %param.27) | copy-start | bytes 6291460
  2.4 23.6 %copy-start.2 = (f32[3,2,128]{0,2,1:T(8,128)}, f32[3,2,128]{0,2,1:T(8,128)S(1)}, u32[]{:S(2)}) copy-start(f32[3,2,128]{0,2,1:T(8,128)S(1)} %copy.42) | copy-start | bytes 9220
  37.0 8.7 %copy-start.3 = (bf16[64,2048]{1,0:T(8,128)(2,1)S(1)}, bf16[64,2048]{1,0:T(8,128)(2,1)}, u32[]{:S(2)}) copy-start(bf16[64,2048]{1,0:T(8,128)(2,1)} %param.17) | copy-start | bytes 786436
  45.7 0.7 copy-start.6
  45.7 1.1 copy-start.4
  45.8 2.4 %copy-start.5 = (f32[64,2]{0,1:T(2,128)S(1)}, f32[64,2]{0,1:T(2,128)}, u32[]{:S(2)}) copy-start(f32[64,2]{0,1:T(2,128)} %param.30) | copy-start | bytes 1540
  125.2 1.4 copy-start.1
where the time goes:
time: 183 us; the launch traced here: 180 us
  Pallas kernels  140 us (77%)
  matrix products  20.2 us (11%)
  other arithmetic  10.5 us (6%)
  local copies, waits for them, and re-layouts  9.21 us (5%)
    pallas_call x6, Pallas kernels, call(): pl.pallas_call(kernel, out_shape=outs, in_specs=[VMEM] * len(args), out_s...  129 us
    pallas_call x1, Pallas kernels, fast_body(): pl.pallas_call(attend_kernel, out_shape=jax.ShapeDtypeStruct((shard_rows,...  11.1 us
    dot_general x1, matrix products, fast_body(): jnp.dot(hidden, down_weight[0], preferred_element_type=jnp.float32)  9.42 us
    dot_general x1, matrix products, fast_body(): jnp.dot(pooled, gate_weight[0], preferred_element_type=jnp.float32)  4.81 us
    unnamed x19, local copies, waits for them, and re-layouts  3.87 us

commit v1 on v0

--- a/solution.py
+++ b/solution.py
@@ -477,143 +477,170 @@
     )[0]
 
 
-def spread_kernel(outer, inner, ys, count, *refs):
-    ins, outs = refs[:count], refs[count : 2 * count]
-    local, send_a, take_a, send_b, take_b, send_c, take_c = refs[2 * count :]
+def expert_kernel(outer, inner, ys, outgoing, gate, up, down, returned, *refs):
+    pooled, answers, half, chip_a, chip_b, from_x, from_y, next_a, next_b = refs[:9]
+    last_a, last_b, final, send, take = refs[9:]
     place, tp = lax.axis_index("sp"), lax.axis_index("tp")
     o, i, y, c = place // inner, place % inner, tp // CORES, tp % CORES
-    steps = [(di, dy) for di in range(inner) for dy in range(ys) if (di, dy) != (0, 0)]
-    mate = (place, y * CORES + 1 - c)
-
-    def beside(di, dy):
-        return (o * inner + (i + di) % inner, (y + dy) % ys * CORES + c)
-
-    def above(d):
-        return ((o + d) % outer * inner + i, tp)
-
-    greet(
-        [above(d) for d in range(1, outer)] + [beside(di, dy) for di, dy in steps] + [mate]
-    )
-
-    def slot(a, core, t, di, dy):
-        return outs[a].at[
-            core, (o - t + outer) % outer, (i - di + inner) % inner, (y - dy + ys) % ys
-        ]
-
-    def first(d, a):
-        return remote(
-            ins[a].at[(o + d) % outer],
-            outs[a].at[c, o, i, y],
-            send_a.at[d, a],
-            take_a.at[d, a],
-            above(d),
-        )
-
-    def second(t, di, dy, a):
-        source = ins[a].at[o] if t == 0 else slot(a, c, t, 0, 0)
-        return remote(
-            source,
-            slot(a, c, t, 0, 0),
-            send_b.at[t, di, dy, a],
-            take_b.at[t, di, dy, a],
-            beside(di, dy),
-        )
-
-    def third(t, di, dy, a):
-        source = ins[a].at[o] if (t, di, dy) == (0, 0, 0) else slot(a, c, t, di, dy)
-        return remote(
-            source, slot(a, c, t, di, dy), send_c.at[t, di, dy, a], take_c.at[t, di, dy, a], mate
-        )
-
-    def landed(where, semaphore):
-        remote(where, where, semaphore, semaphore, mate).wait_recv()
+    far_i, far_y, far_c = (i + 1) % inner, (y + 1) % ys, (c + 1) % CORES
+    features = down.shape[1]
+    cap = outgoing.shape[1]
+    h = cap // 2
+    low, high = pl.ds(0, h), pl.ds(h, h)
+
+    def at(o_, i_, y_, c_):
+        return (o_ * inner + i_, y_ * CORES + c_)
+
+    across, along, mate = at(o, far_i, y, c), at(o, i, far_y, c), at(o, i, y, far_c)
+    greet([at((o + d) % outer, i, y, c) for d in range(1, outer)] + [across, along, mate])
+    started = []
+
+    def push(kind, t, source, target, peer):
+        copy = remote(source, target, send.at[kind, t], take.at[kind, t], peer)
+        copy.start()
+        started.append(copy)
+
+    def landed(kind, t, where):
+        remote(where, where, send.at[kind, t], take.at[kind, t], mate).wait_recv()
+
+    def begin(t):
+        slot = pooled.at[t, c, i, y]
+        source = outgoing.at[o]
+        if t > 0:
+            landed(0, t, slot)
+            source = slot
+        push(1, t, source, slot, across)
+        push(2, t, source, slot, along)
+        push(5, t, source, slot, mate)
 
     def relay(t):
-        for di, dy in steps:
-            for a in range(count):
-                landed(slot(a, c, t, di, dy), take_b.at[t, di, dy, a])
-                third(t, di, dy, a).start()
+        slot = pooled.at[t, c, far_i, y]
+        landed(1, t, slot)
+        part = pooled.at[t, c, far_i, y, low]
+        push(3, t, part, part, along)
+        push(6, t, slot, slot, mate)
+        slot = pooled.at[t, c, i, far_y]
+        landed(2, t, slot)
+        part = pooled.at[t, c, i, far_y, high]
+        push(4, t, part, part, across)
+        push(7, t, slot, slot, mate)
+
+    def corner(t):
+        landed(3, t, pooled.at[t, c, far_i, far_y, low])
+        landed(4, t, pooled.at[t, c, far_i, far_y, high])
+        slot = pooled.at[t, c, far_i, far_y]
+        push(8, t, slot, slot, mate)
+
+    def feed(t):
+        landed(5, t, pooled.at[t, far_c, i, y])
+        landed(6, t, pooled.at[t, far_c, far_i, y])
+        landed(7, t, pooled.at[t, far_c, i, far_y])
+        landed(8, t, pooled.at[t, far_c, far_i, far_y])
+        rows = CORES * inner * ys * cap
+        x = pooled[t, :, :, :, :, :features].reshape(rows, features)
+        extra = pooled[t, :, :, :, :, features:].reshape(rows, -1).astype(jnp.float32)
+        lane = lax.broadcasted_iota(jnp.int32, extra.shape, 1)
+        scale = jnp.sum(jnp.where(lane // 2 == i, extra, 0.0), axis=1, keepdims=True)
+        g = jnp.dot(x, gate[...], preferred_element_type=jnp.float32)
+        u = jnp.dot(x, up[...], preferred_element_type=jnp.float32)
+        hidden = (jax.nn.silu(g) * u).astype(jnp.bfloat16)
+        wide = math.gcd(features, 512)
+        for n in range(features // wide):
+            columns = pl.ds(n * wide, wide)
+            part = jnp.dot(hidden, down[:, columns], preferred_element_type=jnp.float32)
+            answers[t, :, :, :, :, columns] = (
+                (part * scale).astype(jnp.bfloat16).reshape(CORES, inner, ys, cap, wide)
+            )
+        push(9, t, answers.at[t, far_c], half.at[t], mate)
+
+    def gather(t):
+        landed(9, t, half.at[t])
+        for i_ in range(inner):
+            for y_ in range(ys):
+                total = answers[t, c, i_, y_].astype(jnp.float32)
+                total = (total + half[t, i_, y_].astype(jnp.float32)).astype(jnp.bfloat16)
+                chip_a[t, i_, y_] = total[:h]
+                chip_b[t, y_, i_] = total[h:]
+        push(10, t, chip_a.at[t, far_i], from_x.at[t], across)
+        push(11, t, chip_b.at[t, far_y], from_y.at[t], along)
+
+    def add(*parts):
+        total = parts[0].astype(jnp.float32)
+        for part in parts[1:]:
+            total = total + part.astype(jnp.float32)
+        return total.astype(jnp.bfloat16)
+
+    def turn(t):
+        landed(10, t, from_x.at[t])
+        next_a[t] = add(chip_a[t, i, far_y], from_x[t, far_y])
+        push(12, t, next_a.at[t], last_a.at[t], along)
+        landed(11, t, from_y.at[t])
+        next_b[t] = add(chip_b[t, y, far_i], from_y[t, far_i])
+        push(13, t, next_b.at[t], last_b.at[t], across)
+
+    def home(t):
+        landed(12, t, last_a.at[t])
+        landed(13, t, last_b.at[t])
+        target = returned.at[o] if t == 0 else final.at[t]
+        target[:h] = add(chip_a[t, i, y], from_x[t, y], last_a[t])
+        target[h:] = add(chip_b[t, y, i], from_y[t, i], last_b[t])
+        if t > 0:
+            push(14, t, final.at[t], returned.at[o], at((o - t + outer) % outer, i, y, c))
 
     for d in range(1, outer):
-        for a in range(count):
-            first(d, a).start()
-    for t in range(outer):
-        for a in range(count):
-            if t == 0:
-                pltpu.make_async_copy(ins[a].at[o], slot(a, c, 0, 0, 0), local.at[a]).start()
-            else:
-                landed(slot(a, c, t, 0, 0), take_a.at[t, a])
-            for di, dy in reversed(steps):
-                second(t, di, dy, a).start()
-            third(t, 0, 0, a).start()
-        if t > 0:
-            relay(t - 1)
-    relay(outer - 1)
-    for a in range(count):
-        pltpu.make_async_copy(ins[a].at[o], slot(a, c, 0, 0, 0), local.at[a]).wait()
-        for d in range(1, outer):
-            first(d, a).wait_send()
-        for t in range(outer):
-            for di, dy in [(0, 0)] + steps:
-                landed(slot(a, 1 - c, t, di, dy), take_c.at[t, di, dy, a])
-                third(t, di, dy, a).wait_send()
-                if (di, dy) != (0, 0):
-                    second(t, di, dy, a).wait_send()
-
-
-def spread_rows(arrays, outer, inner, ys):
-    count = len(arrays)
-    outs = [
-        jax.ShapeDtypeStruct((CORES, outer, inner, ys) + x.shape[1:], x.dtype) for x in arrays
+        there = (o + d) % outer
+        push(0, d, outgoing.at[there], pooled.at[d, c, i, y], at(there, i, y, c))
+    pooled[0, c, i, y] = outgoing[o]
+    begin(0)
+    begin(1)
+    for k in range(outer + 3):
+        if k < outer:
+            relay(k)
+            if k + 2 < outer:
+                begin(k + 2)
+            corner(k)
+        if 0 <= k - 1 < outer:
+            gather(k - 1)
+        if k < outer:
+            feed(k)
+        if 0 <= k - 3 < outer:
+            home(k - 3)
+        if 0 <= k - 2 < outer:
+            turn(k - 2)
+    for t in range(1, outer):
+        landed(14, t, returned.at[(o + t) % outer])
+    for copy in started:
+        copy.wait_send()
+
+
+def experts(outgoing, gate, up, down, outer, inner, ys):
+    cap, width = outgoing.shape[1:]
+    features = down.shape[1]
+    h = cap // 2
+    kind = jnp.bfloat16
+    scratch = [
+        pltpu.VMEM((outer, CORES, inner, ys, cap, width), kind),
+        pltpu.VMEM((outer, CORES, inner, ys, cap, features), kind),
+        pltpu.VMEM((outer, inner, ys, cap, features), kind),
+        pltpu.VMEM((outer, inner, ys, h, features), kind),
+        pltpu.VMEM((outer, ys, inner, h, features), kind),
+        pltpu.VMEM((outer, ys, h, features), kind),
+        pltpu.VMEM((outer, inner, h, features), kind),
+        pltpu.VMEM((outer, h, features), kind),
+        pltpu.VMEM((outer, h, features), kind),
+        pltpu.VMEM((outer, h, features), kind),
+        pltpu.VMEM((outer, h, features), kind),
+        pltpu.VMEM((outer, cap, features), kind),
+        DMA((15, outer)),
+        DMA((15, outer)),
     ]
-    wide = DMA((outer, inner, ys, count))
-    scratch = [DMA((count,)), DMA((outer, count)), DMA((outer, count)), wide, wide, wide, wide]
     return call(
-        functools.partial(spread_kernel, outer, inner, ys, count), 3, outs, scratch, arrays
-    )
-
-
-def mate_kernel(pieces, source, target, send, take):
-    place, tp = lax.axis_index("sp"), lax.axis_index("tp")
-    y, c = tp // CORES, tp % CORES
-    mate = (place, y * CORES + 1 - c)
-    greet([mate])
-
-    def copy(p):
-        return remote(source.at[1 - c, p], target.at[p], send.at[p], take.at[p], mate)
-
-    for p in range(pieces):
-        copy(p).start()
-    for p in range(pieces):
-        copy(p).wait()
-
-
-def plane_kernel(outer, inner, ys, source, target, send, take):
-    place, tp = lax.axis_index("sp"), lax.axis_index("tp")
-    o, i, y, c = place // inner, place % inner, tp // CORES, tp % CORES
-    steps = [(di, dy) for di in range(inner) for dy in range(ys) if (di, dy) != (0, 0)]
-
-    def beside(di, dy):
-        return (o * inner + (i + di) % inner, (y + dy) % ys * CORES + c)
-
-    greet([beside(di, dy) for di, dy in steps])
-
-    def copy(n, k):
-        di, dy = steps[n]
-        return remote(
-            source.at[k, (i + di) % inner, (y + dy) % ys],
-            target.at[n, k],
-            send.at[n, k],
-            take.at[n, k],
-            beside(di, dy),
-        )
-
-    for k in range(outer):
-        for n in reversed(range(len(steps))):
-            copy(n, k).start()
-    for k in range(outer):
-        for n in range(len(steps)):
-            copy(n, k).wait()
+        functools.partial(expert_kernel, outer, inner, ys),
+        3,
+        [jax.ShapeDtypeStruct((outer, cap, features), kind)],
+        scratch,
+        [outgoing, gate, up, down],
+    )[0]
 
 
 def fast_body(
@@ -640,9 +667,6 @@
     outer = places // inner
     parts = lax.axis_size("tp")
     ys = parts // CORES
-    core = lax.axis_index("tp") % CORES
-    y = lax.axis_index("tp") // CORES
-    i = lax.axis_index("sp") % inner
     own_rows, features = residual.shape
 
     gates = jnp.concatenate([gate_wide, gate_narrow], axis=1).T
@@ -698,53 +722,23 @@
         ),
         axis=1,
     )
-    slot_weight = jnp.sum(jnp.where(picker[:, :, None], of_expert[None, :, :], 0.0), axis=1)
-    slot_weight = jnp.pad(slot_weight, ((0, 0), (0, -inner % 128)))
+    high = of_expert.astype(jnp.bfloat16)
+    rest = (of_expert - high.astype(jnp.float32)).astype(jnp.bfloat16)
+    extra = jnp.stack([high, rest], axis=2).reshape(own_rows, 2 * inner)
+    extra = jnp.pad(extra, ((0, 0), (0, -2 * inner % 128)))
     picker = picker.astype(jnp.bfloat16)
-    outgoing = jnp.dot(picker, normed, preferred_element_type=jnp.float32).astype(jnp.bfloat16)
-    pooled, pooled_weight = spread_rows(
-        [
-            outgoing.reshape(GROUPS, capacity, features),
-            slot_weight.reshape(GROUPS, capacity, slot_weight.shape[1]),
-        ],
+    outgoing = jnp.dot(
+        picker, jnp.concatenate([normed, extra], axis=1), preferred_element_type=jnp.float32
+    ).astype(jnp.bfloat16)
+    returned = experts(
+        outgoing.reshape(GROUPS, capacity, outgoing.shape[1]),
+        gate_weight[0],
+        up_weight[0],
+        down_weight[0],
         outer,
         inner,
         ys,
     )
-    pooled = pooled.reshape(-1, features)
-    pooled_weight = pooled_weight.reshape(pooled.shape[0], -1)
-    scale = jnp.where(i == 0, pooled_weight[:, :1], 0.0)
-    for other in range(1, inner):
-        scale = jnp.where(i == other, pooled_weight[:, other : other + 1], scale)
-    gate_value = jnp.dot(pooled, gate_weight[0], preferred_element_type=jnp.float32)
-    up_value = jnp.dot(pooled, up_weight[0], preferred_element_type=jnp.float32)
-    hidden = (jax.nn.silu(gate_value) * up_value).astype(jnp.bfloat16)
-    answers = jnp.dot(hidden, down_weight[0], preferred_element_type=jnp.float32)
-    answers = (answers * scale).astype(jnp.bfloat16)
-    answers = answers.reshape(CORES, outer, inner, ys, capacity, features)
-    half = jax.ShapeDtypeStruct(answers.shape[1:], jnp.bfloat16)
-    arrived = call(
-        functools.partial(mate_kernel, outer),
-        4,
-        [half],
-        [DMA((outer,)), DMA((outer,))],
-        [answers],
-    )[0]
-    own = lax.dynamic_index_in_dim(answers, core, 0, keepdims=False)
-    chip = (own.astype(jnp.float32) + arrived.astype(jnp.float32)).astype(jnp.bfloat16)
-    others = inner * ys - 1
-    arrived = call(
-        functools.partial(plane_kernel, outer, inner, ys),
-        5,
-        [jax.ShapeDtypeStruct((others, outer, capacity, features), jnp.bfloat16)],
-        [DMA((others, outer)), DMA((others, outer))],
-        [chip],
-    )[0]
-    own = lax.dynamic_slice(
-        chip, (0, i, y, 0, 0), (outer, 1, 1, capacity, features)
-    ).reshape(outer, capacity, features)
-    plane = own.astype(jnp.float32) + jnp.sum(arrived.astype(jnp.float32), axis=0)
-    returned = swap(plane.astype(jnp.bfloat16), "sp", outer, inner, 6)
     combined = jnp.dot(
         picker.T, returned.reshape(-1, features), preferred_element_type=jnp.float32
     )
@@ -754,7 +748,8 @@
 def choose(*args):
     routing, gate_weight = args[12], args[14]
     experts = gate_weight.shape[0] * lax.axis_size("sp")
-    paired = lax.axis_size("tp") % CORES == 0 and gate_weight.shape[0] == 1
+    paired = lax.axis_size("tp") == 2 * CORES and gate_weight.shape[0] == 1
+    paired = paired and routing.shape[1] == 2
     if paired and experts == GROUPS * routing.shape[1]:
         return fast_body(*args)
     return body(*args)

time: 183 us -> 125 us (0.68)
  the two profiles are of different devices: /device:TPU:16 before, /device:TPU:0 now
where the time goes in v1:
time: 125 us
  Pallas kernels  114 us (91%)
  matrix products  5.79 us (5%)
  other arithmetic  2.43 us (2%)
  local copies, waits for them, and re-layouts  2.17 us (2%)
    pallas_call x3, Pallas kernels, call(): pl.pallas_call(kernel, out_shape=outs, in_specs=[VMEM] * len(args), out_s...  111 us
    pallas_call x1, Pallas kernels, fast_body(): pl.pallas_call(attend_kernel, out_shape=jax.ShapeDtypeStruct((shard_rows,...  3.4 us

profile of v1, /device:TPU:0, one launch (start us, length us, event | category | flops | bytes accessed | tf_op | source)
XLA Modules:
  0.0 124.7 jit_solution(2349926299555733053)
XLA Ops:
  0.0 0.0 copy-start
  0.0 0.9 fusion.19
  0.9 0.9 reduce-window.6
  1.8 0.1 slice.20
  1.9 0.1 copy.35
  2.0 0.1 copy.36
  2.1 0.1 broadcast_add_fusion
  2.2 0.1 copy.37
  2.4 0.0 copy-start.1
  2.4 0.1 copy.43
  2.4 0.6 pad.8.clone.refs_4_
  3.1 14.6 %shard_map.163 = (bf16[8,256,128]{2,1,0:T(8,128)(2,1)}, bf16[8,256,128]{2,1,0:T(8,128)(2,1)}, bf16[8,256,128]{2,1,0:T(8,128)(2,1)}, bf16[8,256,128]{2,1,0:T(8,128)(2,1)}, f32[8,8,256]{2,1,0:T(8,128)}) custom-call(bf16[256,128]{1,0:T(8,128)(2,1)} %refs_0_.1, bf16[256,128]{1,0:T(8,128)(2,1)} %refs_1_.1, bf16[256,128]{1,0:T(8,128)(2,1)} %refs_2_.1, ...), custom_call_target="tpu_custom_call" | custom-call | tf_op jit(solution)/shard_map/pallas_call | solution.py:269
  17.6 0.0 copy-done.1
  17.6 3.4 %shard_map.164 = bf16[256,256]{1,0:T(8,128)(2,1)} custom-call(bf16[256,128]{1,0:T(8,128)(2,1)} %qw.1, bf16[256,128]{1,0:T(8,128)(2,1)} %qn.1, f32[256,3]{1,0:T(8,128)} %bitcast.52, bf16[8,256,128]{2,1,0:T(8,128)(2,1)} %get-tuple-element.10.kw, bf16[8,256,128]{2,1,0:T(8,128)(2,1)} %get-tuple-element.11.vw, bf16[8,256,128]{2,1,0:T(8,128)(2,1)} %get-tuple-element.12.kn, ...), custom_call_target="tpu_custom_call" | custom-call | tf_op jit(solution)/shard_map/pallas_call | solution.py:681
  21.0 0.0 copy-start.2
  21.0 5.7 %shard_map.165 = bf16[4,64,256]{2,1,0:T(8,128)(2,1)} custom-call(bf16[4,64,256]{2,1,0:T(8,128)(2,1)} %bitcast.57), custom_call_target="tpu_custom_call" | custom-call | tf_op jit(solution)/shard_map/pallas_call | solution.py:269
  26.8 0.9 slice_bitcast_fusion
  27.6 2.1 %fusion.13 = f32[64,2048]{1,0:T(8,128)S(1)} fusion(bf16[512,2048]{1,0:T(8,128)(2,1)} %param.26, bf16[4,8,8,128]{3,2,1,0:T(8,128)(2,1)S(1)} %get-tuple-element.18), kind=kOutput, calls=%fused_computation.18 | convolution fusion | flops 134217728 | bytes 2686976 | tf_op jit(solution)/shard_map/dot_general | solution.py:704
  29.7 0.0 copy-start.3
  29.7 0.0 copy-done
  29.7 0.0 copy-done.2
  29.8 0.0 copy-start.5
  29.8 0.0 copy-start.4
  29.8 0.6 multiply_reduce_fusion
  30.4 0.0 copy-done.3
  30.4 0.1 multiply_convert_fusion
  30.5 0.0 copy-done.5
  30.6 0.1 fusion.18
  30.6 0.1 reduce_window_sum.28
  30.7 0.2 select_reduce_fusion
  31.0 0.0 copy-done.4
  31.0 0.1 copy.42
  31.1 1.1 convolution_convert_fusion
  32.2 90.5 %shard_map.166 = bf16[4,32,2048]{2,1,0:T(8,128)(2,1)} custom-call(bf16[4,32,2176]{2,1,0:T(8,128)(2,1)} %bitcast.56, bf16[2048,256]{1,0:T(8,128)(2,1)} %bitcast.53, bf16[2048,256]{1,0:T(8,128)(2,1)} %bitcast.54, bf16[256,2048]{1,0:T(8,128)(2,1)} %bitcast.55), custom_call_target="tpu_custom_call" | custom-call | tf_op jit(solution)/shard_map/pallas_call | solution.py:269
  122.7 2.0 %fusion.3 = bf16[64,2048]{1,0:T(8,128)(2,1)} fusion(f32[64,2048]{1,0:T(8,128)S(1)} %get-tuple-element.20, bf16[128,2048]{1,0:T(8,128)(2,1)} %bitcast.50, s32[64]{0:T(128)S(1)} %multiply_add_fusion), kind=kOutput, calls=%fused_computation.6 | convolution fusion | flops 33824768 | bytes 1310976 | tf_op jit(solution)/shard_map/dot_general | solution.py:742
  (11 shorter events, 0.1 us)
Async XLA Ops:
  0.0 29.7 %copy-start = (bf16[512,2048]{1,0:T(8,128)(2,1)S(1)}, bf16[512,2048]{1,0:T(8,128)(2,1)}, u32[]{:S(2)}) copy-start(bf16[512,2048]{1,0:T(8,128)(2,1)} %param.27) | copy-start | bytes 6291460
  2.4 15.3 %copy-start.1 = (f32[3,2,128]{0,2,1:T(8,128)}, f32[3,2,128]{0,2,1:T(8,128)S(1)}, u32[]{:S(2)}) copy-start(f32[3,2,128]{0,2,1:T(8,128)S(1)} %copy.37) | copy-start | bytes 9220
  21.0 8.7 %copy-start.2 = (bf16[64,2048]{1,0:T(8,128)(2,1)S(1)}, bf16[64,2048]{1,0:T(8,128)(2,1)}, u32[]{:S(2)}) copy-start(bf16[64,2048]{1,0:T(8,128)(2,1)} %param.17) | copy-start | bytes 786436
  29.7 0.7 copy-start.3
  29.8 0.8 copy-start.5
  29.8 1.2 copy-start.4

commit v2 on v1

--- a/solution.py
+++ b/solution.py
@@ -265,225 +265,28 @@
     )
 
 
-def call(kernel, number, outs, scratch, args):
-    return pl.pallas_call(
-        kernel,
-        out_shape=outs,
-        in_specs=[VMEM] * len(args),
-        out_specs=[VMEM] * len(outs),
-        scratch_shapes=scratch,
-        compiler_params=pltpu.CompilerParams(collective_id=number, has_side_effects=True),
-    )(*args)
-
-
 DMA = pltpu.SemaphoreType.DMA
 
 
-def keys_kernel(outer, inner, count, *refs):
-    ins, outs = refs[:count], refs[count : 2 * count]
-    local, send_up, take_up, send_in, take_in = refs[2 * count :]
-    place = lax.axis_index("sp")
-    o, i = place // inner, place % inner
-    tp = lax.axis_index("tp")
-
-    def at(o_, i_):
-        return (o_ * inner + i_, tp)
-
-    greet(
-        [at((o + d) % outer, i) for d in range(1, outer)]
-        + [at(o, (i + d) % inner) for d in range(1, inner)]
-    )
-    other = at((o + 1) % outer, i)
-
-    def up(t, a):
-        slot = (o - t) * inner + i
-        source = ins[a] if t == 0 else outs[a].at[slot]
-        return remote(source, outs[a].at[slot], send_up.at[t, a], take_up.at[t, a], at(o + 1, i))
-
-    def across(t, d, a):
-        slot = (o - t) * inner + i
-        source = ins[a] if t == 0 else outs[a].at[slot]
-        return remote(
-            source,
-            outs[a].at[slot],
-            send_in.at[t, d - 1, a],
-            take_in.at[t, d - 1, a],
-            at(o, (i + d) % inner),
-        )
-
-    def landed(slot, a, semaphore):
-        remote(outs[a].at[slot], outs[a].at[slot], semaphore, semaphore, other).wait_recv()
-
-    for a in range(count):
-        pltpu.make_async_copy(ins[a], outs[a].at[place], local.at[a]).start()
-    for t in range(outer):
-
-        @pl.when(o >= t)
-        def _(t=t):
-            for a in range(count):
-                if t > 0:
-                    landed((o - t) * inner + i, a, take_up.at[t - 1, a])
-                if t < outer - 1:
-
-                    @pl.when(o + 1 < outer)
-                    def _(a=a):
-                        up(t, a).start()
-
-                for d in range(1, inner):
-                    if t > 0:
-                        across(t, d, a).start()
-                    else:
-
-                        @pl.when((i + d) % inner > i)
-                        def _(a=a, d=d):
-                            across(t, d, a).start()
-
-    for t in range(outer):
-
-        @pl.when(o >= t)
-        def _(t=t):
-            for a in range(count):
-                for d in range(1, inner):
-                    giver = (i - d + inner) % inner
-                    slot = (o - t) * inner + giver
-                    if t > 0:
-                        landed(slot, a, take_in.at[t, d - 1, a])
-                        across(t, d, a).wait_send()
-                    else:
-
-                        @pl.when(giver < i)
-                        def _(a=a, d=d, slot=slot):
-                            landed(slot, a, take_in.at[0, d - 1, a])
-
-                        @pl.when((i + d) % inner > i)
-                        def _(a=a, d=d):
-                            across(0, d, a).wait_send()
-
-                if t < outer - 1:
-
-                    @pl.when(o + 1 < outer)
-                    def _(a=a):
-                        up(t, a).wait_send()
-
-    for a in range(count):
-        pltpu.make_async_copy(ins[a], outs[a].at[place], local.at[a]).wait()
-
-
-def gather_keys(arrays, outer, inner):
-    count = len(arrays)
-    outs = [jax.ShapeDtypeStruct((outer * inner,) + x.shape, x.dtype) for x in arrays]
-    scratch = [
-        DMA((count,)),
-        DMA((outer, count)),
-        DMA((outer, count)),
-        DMA((outer, inner, count)),
-        DMA((outer, inner, count)),
-    ]
-    return call(functools.partial(keys_kernel, outer, inner, count), 1, outs, scratch, arrays)
-
-
-def attend_kernel(qw, qn, near, kw, vw, kn, vn, far, out, top, total, mixed):
-    place = lax.axis_index("sp")
-    rows = qw.shape[0]
-    width = qn.shape[1]
-    heads = 1 + width // HN
-    lanes = lax.broadcasted_iota(jnp.int32, (rows, width), 1) // HN
-
-    def query(h):
-        if h == 0:
-            return qw[...]
-        return jnp.where(lanes == h - 1, qn[...], jnp.zeros_like(qn[...]))
-
-    def block(j, shift, diagonal):
-        for h in range(heads):
-            keys, values = (kw, vw) if h == 0 else (kn, vn)
-            size = HW if h == 0 else HN
-            scores = lax.dot_general(
-                query(h), keys[j], (((1,), (1,)), ((), ())), preferred_element_type=jnp.float32
-            )
-            drop = (near[:, h : h + 1] + shift[h]) - far[j, h : h + 1, :]
-            scores = scores * size ** (-0.5) + drop
-            if diagonal:
-                t = lax.broadcasted_iota(jnp.int32, scores.shape, 0)
-                s = lax.broadcasted_iota(jnp.int32, scores.shape, 1)
-                scores = jnp.where(s <= t, scores, -jnp.inf)
-            peak = jnp.max(scores, axis=1, keepdims=True)
-            if diagonal:
-                weights = jnp.exp(scores - peak)
-                total[h] = jnp.sum(weights, axis=1, keepdims=True)
-                mixed[h] = jnp.dot(
-                    weights.astype(jnp.bfloat16), values[j], preferred_element_type=jnp.float32
-                )
-                top[h] = peak
-            else:
-                before = top[h]
-                peak = jnp.maximum(before, peak)
-                weights = jnp.exp(scores - peak)
-                shrink = jnp.exp(before - peak)
-                total[h] = total[h] * shrink + jnp.sum(weights, axis=1, keepdims=True)
-                mixed[h] = mixed[h] * shrink + jnp.dot(
-                    weights.astype(jnp.bfloat16), values[j], preferred_element_type=jnp.float32
-                )
-                top[h] = peak
-
-    block(place, [jnp.zeros((1, 1), jnp.float32)] * heads, True)
-
-    def step(t, shift):
-        j = place - 1 - t
-        shift = tuple(shift[h] + far[j, h : h + 1, rows - 1 : rows] for h in range(heads))
-        block(j, shift, False)
-        return shift
-
-    lax.fori_loop(0, place, step, tuple(jnp.zeros((1, 1), jnp.float32) for _ in range(heads)))
-    out[:, : qw.shape[1]] = (mixed[0] / total[0]).astype(jnp.bfloat16)
-    narrow = mixed[1] / total[1]
-    for h in range(2, heads):
-        narrow = jnp.where(lanes == h - 1, mixed[h] / total[h], narrow)
-    out[:, qw.shape[1] :] = narrow.astype(jnp.bfloat16)
-
-
-def swap_kernel(axis, n, stride, source, target, local, send, take):
-    sp, tp = lax.axis_index("sp"), lax.axis_index("tp")
-    me = (sp if axis == "sp" else tp) // stride
-    rest = (sp if axis == "sp" else tp) % stride
-
-    def at(k):
-        return (k * stride + rest, tp) if axis == "sp" else (sp, k * stride + rest)
-
-    greet([at((me + d) % n) for d in range(1, n)])
-
-    def copy(d):
-        k = (me + d) % n
-        return remote(source.at[k], target.at[me], send.at[d], take.at[d], at(k))
-
-    for d in range(1, n):
-        copy(d).start()
-    own = pltpu.make_async_copy(source.at[me], target.at[me], local.at[0])
-    own.start()
-    own.wait()
-    for d in range(1, n):
-        slot = target.at[(me - d + n) % n]
-        remote(slot, slot, send.at[d], take.at[d], at((me + d) % n)).wait_recv()
-        copy(d).wait_send()
-
-
-def swap(array, axis, n, stride, number):
-    return call(
-        functools.partial(swap_kernel, axis, n, stride),
-        number,
-        [jax.ShapeDtypeStruct(array.shape, array.dtype)],
-        [DMA((1,)), DMA((n,)), DMA((n,))],
-        [array],
-    )[0]
-
-
-def expert_kernel(outer, inner, ys, outgoing, gate, up, down, returned, *refs):
-    pooled, answers, half, chip_a, chip_b, from_x, from_y, next_a, next_b = refs[:9]
-    last_a, last_b, final, send, take = refs[9:]
+LOG2E = math.log2(math.e)
+
+
+def layer_kernel(outer, inner, ys, *refs):
+    gates, qw, kw, vw, qn, kn, vn, residual, gain, picker, extra = refs[:11]
+    out_wide, out_narrow, gate_hbm, up_hbm, down_hbm, result = refs[11:17]
+    kws, vws, kns, vns, far, run, peak, total, acc_w, acc_n, att, swapped = refs[17:29]
+    wide_w, narrow_w, gate, up, down, middle, outgoing, returned = refs[29:37]
+    pooled, answers, half, chip_a, chip_b, from_x, from_y, next_a, next_b = refs[37:46]
+    last_a, last_b, final = refs[46:49]
+    load, lift_s, lift_r, cross_s, cross_r, far_s, far_r, swap_s, swap_r, send, take = refs[49:]
     place, tp = lax.axis_index("sp"), lax.axis_index("tp")
     o, i, y, c = place // inner, place % inner, tp // CORES, tp % CORES
     far_i, far_y, far_c = (i + 1) % inner, (y + 1) % ys, (c + 1) % CORES
-    features = down.shape[1]
+    places, parts = outer * inner, ys * CORES
+    rows, wide = qw.shape
+    narrow = qn.shape[1]
+    heads = 1 + narrow // HN
+    own_rows, features = residual.shape
     cap = outgoing.shape[1]
     h = cap // 2
     low, high = pl.ds(0, h), pl.ds(h, h)
@@ -492,7 +295,219 @@
         return (o_ * inner + i_, y_ * CORES + c_)
 
     across, along, mate = at(o, far_i, y, c), at(o, i, far_y, c), at(o, i, y, far_c)
-    greet([at((o + d) % outer, i, y, c) for d in range(1, outer)] + [across, along, mate])
+
+    loads = [
+        pltpu.make_async_copy(source, target, load.at[n])
+        for n, (source, target) in enumerate(
+            [
+                (out_wide, wide_w),
+                (out_narrow, narrow_w),
+                (gate_hbm.at[0], gate),
+                (up_hbm.at[0], up),
+                (down_hbm.at[0], down),
+            ]
+        )
+    ]
+    for copy in loads:
+        copy.start()
+    far[...] = jnp.zeros_like(far)
+    greet(
+        [((place + d) % places, tp) for d in range(1, places)]
+        + [(place, (tp + d) % parts) for d in range(1, parts)]
+    )
+
+    ins, blocks = (kw, vw, kn, vn), (kws, vws, kns, vns)
+    count = len(ins)
+
+    def source_of(t, a):
+        slot = (o - t) * inner + i
+        return (ins[a] if t == 0 else blocks[a].at[slot]), blocks[a].at[slot]
+
+    def lift(t, a):
+        source, target = source_of(t, a)
+        return remote(
+            source, target, lift_s.at[t, a], lift_r.at[t, a], at(o + 1, i, y, c)
+        )
+
+    def cross(t, a):
+        source, target = source_of(t, a)
+        return remote(source, target, cross_s.at[t, a], cross_r.at[t, a], across)
+
+    def arrived(where, semaphore):
+        remote(where, where, semaphore, semaphore, mate).wait_recv()
+
+    for a in range(count):
+
+        @pl.when(o + 1 < outer)
+        def _(a=a):
+            lift(0, a).start()
+
+        @pl.when(i < far_i)
+        def _(a=a):
+            cross(0, a).start()
+
+    x = gates[...]
+    step = jnp.minimum(x, 0.0) - jnp.log1p(jnp.exp(-jnp.abs(x)))
+    lane = lax.broadcasted_iota(jnp.int32, step.shape, 1)
+    shift = 1
+    while shift < rows:
+        step = step + jnp.where(lane >= shift, pltpu.roll(step, shift, 1), 0.0)
+        shift *= 2
+    run[...] = step
+    near = step * LOG2E
+
+    head_lane = lax.broadcasted_iota(jnp.int32, (rows, narrow), 1) // HN
+
+    def attend(block_of, decay, diagonal):
+        columns = jnp.transpose(decay * LOG2E)
+        for n in range(heads):
+            k, v = (block_of(0), block_of(1)) if n == 0 else (block_of(2), block_of(3))
+            if n == 0:
+                q, size = qw[...], HW
+            else:
+                q, size = jnp.where(head_lane == n - 1, qn[...], jnp.zeros_like(qn[...])), HN
+            s = lax.dot_general(k, q, (((1,), (1,)), ((), ())), preferred_element_type=jnp.float32)
+            s = s * (LOG2E * size ** (-0.5)) - columns[:, n : n + 1]
+            if diagonal:
+                key = lax.broadcasted_iota(jnp.int32, s.shape, 0)
+                query = lax.broadcasted_iota(jnp.int32, s.shape, 1)
+                s = jnp.where(key <= query, s, -jnp.inf)
+            row = near[n : n + 1]
+            new = jnp.max(s, axis=0, keepdims=True) + row
+            if not diagonal:
+                before = peak[n : n + 1]
+                new = jnp.maximum(new, before)
+            weights = jnp.exp2(s - (new - row))
+            mass = jnp.sum(weights, axis=0, keepdims=True)
+            part = lax.dot_general(
+                v if n == 0 else v[:, (n - 1) * HN : n * HN],
+                weights.astype(jnp.bfloat16),
+                (((0,), (0,)), ((), ())),
+                preferred_element_type=jnp.float32,
+            )
+            acc = acc_w if n == 0 else acc_n.at[(n - 1) * HN : n * HN]
+            if diagonal:
+                total[n : n + 1] = mass
+                acc[...] = part
+            else:
+                shrink = jnp.exp2(before - new)
+                total[n : n + 1] = total[n : n + 1] * shrink + mass
+                acc[...] = acc[...] * shrink + part
+            peak[n : n + 1] = new
+
+    attend(lambda a: ins[a][...], step, True)
+    for d in range(1, places):
+
+        @pl.when(place + d < places)
+        def _(d=d):
+            remote(run, far.at[place], far_s.at[d], far_r.at[d], (place + d, tp)).start()
+
+    for d in range(1, places):
+
+        @pl.when(place >= d)
+        def _(d=d):
+            arrived(far.at[place - d], far_r.at[d])
+
+    def visit(slot):
+        offset = jnp.zeros((far.shape[1], 1), jnp.float32)
+        for b in range(places):
+            inside = jnp.logical_and(b >= slot, b < place)
+            offset = offset + jnp.where(inside, far[b, :, rows - 1 : rows], 0.0)
+        attend(lambda a: blocks[a][slot], far[slot] - offset, False)
+
+    def relay(t):
+        @pl.when(o >= t)
+        def _():
+            for a in range(count):
+                arrived(blocks[a].at[(o - t) * inner + i], lift_r.at[t - 1, a])
+                if t < outer - 1:
+
+                    @pl.when(o + 1 < outer)
+                    def _(a=a):
+                        lift(t, a).start()
+
+                cross(t, a).start()
+
+    def own(t):
+        @pl.when(o >= t)
+        def _():
+            visit((o - t) * inner + i)
+
+    def other(t):
+        @pl.when((o >= t) if t > 0 else (far_i < i))
+        def _():
+            slot = (o - t) * inner + far_i
+            for a in range(count):
+                arrived(blocks[a].at[slot], cross_r.at[t, a])
+            visit(slot)
+
+    for t in range(outer):
+        if t > 0:
+            own(t)
+        if t + 1 < outer:
+            relay(t + 1)
+        other(t)
+
+    mixed = jnp.transpose(acc_w[...] / total[0:1]).astype(jnp.bfloat16)
+    att[:, :, :wide] = mixed.reshape(parts, own_rows, wide)
+    for n in range(1, heads):
+        piece = slice((n - 1) * HN, n * HN)
+        acc_n[piece] = acc_n[piece] / total[n : n + 1]
+    mixed = jnp.transpose(acc_n[...]).astype(jnp.bfloat16)
+    att[:, :, wide:] = mixed.reshape(parts, own_rows, narrow)
+
+    def swap(d):
+        k = (tp + d) % parts
+        return remote(att.at[k], swapped.at[tp], swap_s.at[d], swap_r.at[d], (place, k))
+
+    for d in range(1, parts):
+        swap(d).start()
+    swapped[tp] = att[tp]
+    for t in range(outer):
+        for a in range(count):
+            if t < outer - 1:
+
+                @pl.when(jnp.logical_and(o >= t, o + 1 < outer))
+                def _(t=t, a=a):
+                    lift(t, a).wait_send()
+
+            @pl.when((o >= t) if t > 0 else (i < far_i))
+            def _(t=t, a=a):
+                cross(t, a).wait_send()
+
+    for d in range(1, places):
+
+        @pl.when(place + d < places)
+        def _(d=d):
+            remote(run, far.at[place], far_s.at[d], far_r.at[d], (place + d, tp)).wait_send()
+
+    loads[0].wait()
+    loads[1].wait()
+    for d in range(1, parts):
+        arrived(swapped.at[(tp - d + parts) % parts], swap_r.at[d])
+        swap(d).wait_send()
+    rows_w = jnp.concatenate([swapped[p, :, :wide] for p in range(parts)], axis=1)
+    rows_n = jnp.concatenate([swapped[p, :, wide:] for p in range(parts)], axis=1)
+    tile = math.gcd(features, 512)
+    squares = jnp.zeros((own_rows, 1), jnp.float32)
+    for n in range(features // tile):
+        at_n = pl.ds(n * tile, tile)
+        part = jnp.dot(rows_w, wide_w[:, at_n], preferred_element_type=jnp.float32)
+        part = part + jnp.dot(rows_n, narrow_w[:, at_n], preferred_element_type=jnp.float32)
+        part = (residual[:, at_n].astype(jnp.float32) + part).astype(jnp.bfloat16)
+        middle[:, at_n] = part
+        part = part.astype(jnp.float32)
+        squares = squares + jnp.sum(part * part, axis=1, keepdims=True)
+    factor = lax.rsqrt(squares / features + epsilon)
+    pick = picker[...]
+    for n in range(features // tile):
+        at_n = pl.ds(n * tile, tile)
+        part = middle[:, at_n].astype(jnp.float32) * factor * gain[:, at_n]
+        part = jnp.dot(pick, part.astype(jnp.bfloat16), preferred_element_type=jnp.float32)
+        outgoing[:, :, at_n] = part.astype(jnp.bfloat16).reshape(GROUPS, cap, tile)
+    part = jnp.dot(pick, extra[...], preferred_element_type=jnp.float32)
+    outgoing[:, :, features:] = part.astype(jnp.bfloat16).reshape(GROUPS, cap, extra.shape[1])
+
     started = []
 
     def push(kind, t, source, target, peer):
@@ -501,7 +516,7 @@
         started.append(copy)
 
     def landed(kind, t, where):
-        remote(where, where, send.at[kind, t], take.at[kind, t], mate).wait_recv()
+        arrived(where, take.at[kind, t])
 
     def begin(t):
         slot = pooled.at[t, c, i, y]
@@ -541,6 +556,9 @@
         extra = pooled[t, :, :, :, :, features:].reshape(rows, -1).astype(jnp.float32)
         lane = lax.broadcasted_iota(jnp.int32, extra.shape, 1)
         scale = jnp.sum(jnp.where(lane // 2 == i, extra, 0.0), axis=1, keepdims=True)
+        if t == 0:
+            for copy in loads[2:]:
+                copy.wait()
         g = jnp.dot(x, gate[...], preferred_element_type=jnp.float32)
         u = jnp.dot(x, up[...], preferred_element_type=jnp.float32)
         hidden = (jax.nn.silu(g) * u).astype(jnp.bfloat16)
@@ -611,36 +629,11 @@
         landed(14, t, returned.at[(o + t) % outer])
     for copy in started:
         copy.wait_send()
-
-
-def experts(outgoing, gate, up, down, outer, inner, ys):
-    cap, width = outgoing.shape[1:]
-    features = down.shape[1]
-    h = cap // 2
-    kind = jnp.bfloat16
-    scratch = [
-        pltpu.VMEM((outer, CORES, inner, ys, cap, width), kind),
-        pltpu.VMEM((outer, CORES, inner, ys, cap, features), kind),
-        pltpu.VMEM((outer, inner, ys, cap, features), kind),
-        pltpu.VMEM((outer, inner, ys, h, features), kind),
-        pltpu.VMEM((outer, ys, inner, h, features), kind),
-        pltpu.VMEM((outer, ys, h, features), kind),
-        pltpu.VMEM((outer, inner, h, features), kind),
-        pltpu.VMEM((outer, h, features), kind),
-        pltpu.VMEM((outer, h, features), kind),
-        pltpu.VMEM((outer, h, features), kind),
-        pltpu.VMEM((outer, h, features), kind),
-        pltpu.VMEM((outer, cap, features), kind),
-        DMA((15, outer)),
-        DMA((15, outer)),
-    ]
-    return call(
-        functools.partial(expert_kernel, outer, inner, ys),
-        3,
-        [jax.ShapeDtypeStruct((outer, cap, features), kind)],
-        scratch,
-        [outgoing, gate, up, down],
-    )[0]
+    slots = returned[...].reshape(GROUPS * cap, features)
+    combined = lax.dot_general(
+        pick, slots, (((0,), (0,)), ((), ())), preferred_element_type=jnp.float32
+    )
+    result[...] = (middle[...].astype(jnp.float32) + combined).astype(jnp.bfloat16)
 
 
 def fast_body(
@@ -668,52 +661,18 @@
     parts = lax.axis_size("tp")
     ys = parts // CORES
     own_rows, features = residual.shape
-
     gates = jnp.concatenate([gate_wide, gate_narrow], axis=1).T
-    running = jnp.cumsum(jax.nn.log_sigmoid(gates), axis=1)
-    heads = gates.shape[0]
-    far = jnp.pad(running, ((0, -heads % 8), (0, 0)))
-    keys_wide, values_wide, keys_narrow, values_narrow, far = gather_keys(
-        [key_wide, value_wide, key_narrow, value_narrow, far], outer, inner
-    )
-    shard_rows, wide = query_wide.shape
+    gates = jnp.pad(gates, ((0, -gates.shape[0] % 8), (0, 0)))
+    rows, wide = query_wide.shape
     narrow = query_narrow.shape[1]
-    att = pl.pallas_call(
-        attend_kernel,
-        out_shape=jax.ShapeDtypeStruct((shard_rows, wide + narrow), jnp.bfloat16),
-        in_specs=[VMEM] * 8,
-        out_specs=VMEM,
-        scratch_shapes=[
-            pltpu.VMEM((heads, shard_rows, 1), jnp.float32),
-            pltpu.VMEM((heads, shard_rows, 1), jnp.float32),
-            pltpu.VMEM((heads, shard_rows, wide), jnp.float32),
-        ],
-    )(
-        query_wide,
-        query_narrow,
-        running.T,
-        keys_wide,
-        values_wide,
-        keys_narrow,
-        values_narrow,
-        far,
-    )
-    att = swap(att.reshape(parts, own_rows, wide + narrow), "tp", parts, 1, 2)
-    att_wide = jnp.transpose(att[:, :, :wide], (1, 0, 2)).reshape(own_rows, parts * wide)
-    att_narrow = jnp.transpose(att[:, :, wide:], (1, 0, 2)).reshape(own_rows, parts * narrow)
-    mixed = jnp.dot(att_wide, out_wide, preferred_element_type=jnp.float32)
-    mixed = mixed + jnp.dot(att_narrow, out_narrow, preferred_element_type=jnp.float32)
-    middle = (residual.astype(jnp.float32) + mixed).astype(jnp.bfloat16)
-    middle_wide = middle.astype(jnp.float32)
-    spread = jnp.mean(middle_wide * middle_wide, axis=1, keepdims=True)
-    normed = (middle_wide * lax.rsqrt(spread + epsilon) * norm_gain).astype(jnp.bfloat16)
-
-    capacity = own_rows * GROUPS // places
+
+    cap = own_rows * GROUPS // places
     group = routing[:, 0] // inner
     matches = (group[:, None] == jnp.arange(GROUPS, dtype=jnp.int32)[None, :]).astype(jnp.int32)
     ranking = jnp.sum((jnp.cumsum(matches, axis=0) - matches) * matches, axis=1)
-    placing = group * capacity + ranking
-    picker = placing[None, :] == jnp.arange(GROUPS * capacity, dtype=jnp.int32)[:, None]
+    placing = group * cap + ranking
+    picker = placing[None, :] == jnp.arange(GROUPS * cap, dtype=jnp.int32)[:, None]
+    picker = picker.astype(jnp.bfloat16)
     of_expert = jnp.sum(
         jnp.where(
             (routing % inner)[:, :, None] == jnp.arange(inner, dtype=jnp.int32)[None, None, :],
@@ -726,23 +685,87 @@
     rest = (of_expert - high.astype(jnp.float32)).astype(jnp.bfloat16)
     extra = jnp.stack([high, rest], axis=2).reshape(own_rows, 2 * inner)
     extra = jnp.pad(extra, ((0, 0), (0, -2 * inner % 128)))
-    picker = picker.astype(jnp.bfloat16)
-    outgoing = jnp.dot(
-        picker, jnp.concatenate([normed, extra], axis=1), preferred_element_type=jnp.float32
-    ).astype(jnp.bfloat16)
-    returned = experts(
-        outgoing.reshape(GROUPS, capacity, outgoing.shape[1]),
-        gate_weight[0],
-        up_weight[0],
-        down_weight[0],
-        outer,
-        inner,
-        ys,
-    )
-    combined = jnp.dot(
-        picker.T, returned.reshape(-1, features), preferred_element_type=jnp.float32
-    )
-    return (middle_wide + combined).astype(jnp.bfloat16)
+
+    h = cap // 2
+    width = features + extra.shape[1]
+    kind, full = jnp.bfloat16, jnp.float32
+
+    def vmem(*shape, dtype=kind):
+        return pltpu.VMEM(shape, dtype)
+
+    scratch = [
+        vmem(places, rows, wide),
+        vmem(places, rows, wide),
+        vmem(places, rows, narrow),
+        vmem(places, rows, narrow),
+        vmem(places, gates.shape[0], rows, dtype=full),
+        vmem(gates.shape[0], rows, dtype=full),
+        vmem(gates.shape[0], rows, dtype=full),
+        vmem(gates.shape[0], rows, dtype=full),
+        vmem(wide, rows, dtype=full),
+        vmem(narrow, rows, dtype=full),
+        vmem(parts, own_rows, wide + narrow),
+        vmem(parts, own_rows, wide + narrow),
+        vmem(*out_wide.shape),
+        vmem(*out_narrow.shape),
+        vmem(*gate_weight.shape[1:]),
+        vmem(*up_weight.shape[1:]),
+        vmem(*down_weight.shape[1:]),
+        vmem(own_rows, features),
+        vmem(GROUPS, cap, width),
+        vmem(outer, cap, features),
+        vmem(outer, CORES, inner, ys, cap, width),
+        vmem(outer, CORES, inner, ys, cap, features),
+        vmem(outer, inner, ys, cap, features),
+        vmem(outer, inner, ys, h, features),
+        vmem(outer, ys, inner, h, features),
+        vmem(outer, ys, h, features),
+        vmem(outer, inner, h, features),
+        vmem(outer, h, features),
+        vmem(outer, h, features),
+        vmem(outer, h, features),
+        vmem(outer, h, features),
+        vmem(outer, cap, features),
+        DMA((5,)),
+        DMA((outer, 4)),
+        DMA((outer, 4)),
+        DMA((outer, 4)),
+        DMA((outer, 4)),
+        DMA((places,)),
+        DMA((places,)),
+        DMA((parts,)),
+        DMA((parts,)),
+        DMA((15, outer)),
+        DMA((15, outer)),
+    ]
+    anywhere = pl.BlockSpec(memory_space=pl.ANY)
+    return pl.pallas_call(
+        functools.partial(layer_kernel, outer, inner, ys),
+        out_shape=jax.ShapeDtypeStruct(residual.shape, residual.dtype),
+        in_specs=[VMEM] * 11 + [anywhere] * 5,
+        out_specs=VMEM,
+        scratch_shapes=scratch,
+        compiler_params=pltpu.CompilerParams(
+            collective_id=1, has_side_effects=True, vmem_limit_bytes=56 * 1024 * 1024
+        ),
+    )(
+        gates,
+        query_wide,
+        key_wide,
+        value_wide,
+        query_narrow,
+        key_narrow,
+        value_narrow,
+        residual,
+        norm_gain[None, :],
+        picker,
+        extra,
+        out_wide,
+        out_narrow,
+        gate_weight,
+        up_weight,
+        down_weight,
+    )
 
 
 def choose(*args):

time: 125 us -> 101 us (0.81)
  the two profiles are of different devices: /device:TPU:0 before, /device:TPU:16 now
where the time goes in v2:
time: 101 us; the launch traced here: 100 us
  Pallas kernels  92.8 us (92%)
  other arithmetic  4.46 us (4%)
  local copies, waits for them, and re-layouts  3 us (3%)
    pallas_call x1, Pallas kernels, fast_body(): pl.pallas_call(functools.partial(layer_kernel, outer, inner, ys), out_sha...  92.8 us

profile of v2, /device:TPU:16, one launch (start us, length us, event | category | flops | bytes accessed | tf_op | source)
XLA Modules:
  0.0 100.3 jit_solution(12879515432060834624)
XLA Ops:
  0.0 0.7 fusion.5
  0.7 0.7 and_select_fusion
  1.4 0.7 fusion.2
  2.1 0.7 maximum_bitcast_fusion
  2.8 0.6 pad.8.refs_0_
  3.4 0.1 copy.26
  3.5 0.6 pad.9.refs_10_
  4.1 0.1 fusion.1
  4.2 0.1 reduce_window_sum.11
  4.3 0.2 select_reduce_fusion
  4.5 0.7 multiply_add_fusion
  5.2 0.6 fusion.refs_9_
  5.8 92.8 %shard_map.163 = bf16[64,2048]{1,0:T(8,128)(2,1)} custom-call(f32[8,256]{1,0:T(8,128)} %pad.8.refs_0_, bf16[256,128]{1,0:T(8,128)(2,1)} %refs_1_.1, bf16[256,128]{1,0:T(8,128)(2,1)} %refs_2_.1, bf16[256,128]{1,0:T(8,128)(2,1)} %refs_3_.1, bf16[256,128]{1,0:T(8,128)(2,1)} %refs_4_.1, bf16[256,128]{1,0:T(8,128)(2,1)} %refs_5_.1, bf16[256,128]{1,0:T(8,128)(2,1)} %refs_6_.1, ...), custom_call_target="tpu_custom_call" | custom-call | tf_op jit(solution)/shard_map/pallas_call | solution.py:742
  98.6 1.7 %copy.28 = bf16[64,2048]{1,0:T(8,128)(2,1)} copy(bf16[64,2048]{1,0:T(8,128)(2,1)} %shard_map.163) | data formatting | bytes 524288
  (3 shorter events, 0.0 us)

commit v3 on v2

--- a/solution.py
+++ b/solution.py
@@ -272,13 +272,15 @@
 
 
 def layer_kernel(outer, inner, ys, *refs):
-    gates, qw, kw, vw, qn, kn, vn, residual, gain, picker, extra = refs[:11]
-    out_wide, out_narrow, gate_hbm, up_hbm, down_hbm, result = refs[11:17]
-    kws, vws, kns, vns, far, run, peak, total, acc_w, acc_n, att, swapped = refs[17:29]
-    wide_w, narrow_w, gate, up, down, middle, outgoing, returned = refs[29:37]
-    pooled, answers, half, chip_a, chip_b, from_x, from_y, next_a, next_b = refs[37:46]
-    last_a, last_b, final = refs[46:49]
-    load, lift_s, lift_r, cross_s, cross_r, far_s, far_r, swap_s, swap_r, send, take = refs[49:]
+    gate_w, gate_n, chosen, shares, qw, kw, vw, qn, kn, vn, residual, gain = refs[:12]
+    out_wide, out_narrow, gate_hbm, up_hbm, down_hbm, result = refs[12:18]
+    refs = refs[3:]
+    kws, vws, kns, vns, far, run, peak, total, acc_w, acc_n, att, swapped = refs[15:27]
+    wide_w, narrow_w, gate, up, down, middle, outgoing, returned = refs[27:35]
+    pooled, answers, half, chip_a, chip_b, from_x, from_y, next_a, next_b = refs[35:44]
+    last_a, last_b, final, picker, board, factor = refs[44:50]
+    load, lift_s, lift_r, cross_s, cross_r, turn_s, turn_r = refs[50:57]
+    far_s, far_r, swap_s, swap_r, send, take = refs[57:]
     place, tp = lax.axis_index("sp"), lax.axis_index("tp")
     o, i, y, c = place // inner, place % inner, tp // CORES, tp % CORES
     far_i, far_y, far_c = (i + 1) % inner, (y + 1) % ys, (c + 1) % CORES
@@ -311,43 +313,19 @@
     for copy in loads:
         copy.start()
     far[...] = jnp.zeros_like(far)
-    greet(
-        [((place + d) % places, tp) for d in range(1, places)]
-        + [(place, (tp + d) % parts) for d in range(1, parts)]
-    )
-
-    ins, blocks = (kw, vw, kn, vn), (kws, vws, kns, vns)
-    count = len(ins)
-
-    def source_of(t, a):
-        slot = (o - t) * inner + i
-        return (ins[a] if t == 0 else blocks[a].at[slot]), blocks[a].at[slot]
-
-    def lift(t, a):
-        source, target = source_of(t, a)
-        return remote(
-            source, target, lift_s.at[t, a], lift_r.at[t, a], at(o + 1, i, y, c)
-        )
-
-    def cross(t, a):
-        source, target = source_of(t, a)
-        return remote(source, target, cross_s.at[t, a], cross_r.at[t, a], across)
-
-    def arrived(where, semaphore):
-        remote(where, where, semaphore, semaphore, mate).wait_recv()
-
-    for a in range(count):
-
-        @pl.when(o + 1 < outer)
-        def _(a=a):
-            lift(0, a).start()
-
-        @pl.when(i < far_i)
-        def _(a=a):
-            cross(0, a).start()
-
-    x = gates[...]
-    step = jnp.minimum(x, 0.0) - jnp.log1p(jnp.exp(-jnp.abs(x)))
+    peers = [((place + d) % places, tp) for d in range(1, places)]
+    peers = peers + [(place, (tp + d) % parts) for d in range(1, parts)]
+    barrier = pltpu.get_barrier_semaphore()
+    for peer in peers:
+        pl.semaphore_signal(barrier, inc=1, device_id=peer, device_id_type=MESH)
+    picks = chosen.shape[0]
+    board[...] = jnp.zeros_like(board)
+    board[:1] = gate_w[...]
+    board[1:heads] = gate_n[...]
+    board[heads : heads + picks, :own_rows] = chosen[...].astype(jnp.float32)
+    board[heads + picks : heads + 2 * picks, :own_rows] = shares[...]
+    facts = board[...]
+    step = jnp.minimum(facts, 0.0) - jnp.log1p(jnp.exp(-jnp.abs(facts)))
     lane = lax.broadcasted_iota(jnp.int32, step.shape, 1)
     shift = 1
     while shift < rows:
@@ -355,6 +333,54 @@
         shift *= 2
     run[...] = step
     near = step * LOG2E
+    pl.semaphore_wait(barrier, len(peers))
+    for d in range(1, places):
+
+        @pl.when(place + d < places)
+        def _(d=d):
+            remote(run, far.at[place], far_s.at[d], far_r.at[d], (place + d, tp)).start()
+
+    ins, blocks = (kw, vw, kn, vn), (kws, vws, kns, vns)
+    count = len(ins)
+
+    def source_of(t, a):
+        slot = (o - t) * inner + i
+        return (ins[a] if t == 0 else blocks[a].at[slot]), blocks[a].at[slot]
+
+    def lift(t, a):
+        source, target = source_of(t, a)
+        return remote(
+            source, target, lift_s.at[t, a], lift_r.at[t, a], at(o + 1, i, y, c)
+        )
+
+    def cross(t, a):
+        source, target = source_of(t, a)
+        return remote(source, target, cross_s.at[t, a], cross_r.at[t, a], across)
+
+    def arrived(where, semaphore):
+        remote(where, where, semaphore, semaphore, mate).wait_recv()
+
+    def detour(a):
+        slot = blocks[a].at[far_i]
+        return remote(slot, slot, turn_s.at[a], turn_r.at[a], at(o + 1, i, y, c))
+
+    def detours(a):
+        return a >= count // 2
+
+    def crosses(t, a):
+        if t == 0:
+            return jnp.logical_or(i < far_i, o == 0) if detours(a) else i < far_i
+        return o > t if detours(a) else o >= t
+
+    for a in range(count):
+
+        @pl.when(o + 1 < outer)
+        def _(a=a):
+            lift(0, a).start()
+
+        @pl.when(crosses(0, a))
+        def _(a=a):
+            cross(0, a).start()
 
     head_lane = lax.broadcasted_iota(jnp.int32, (rows, narrow), 1) // HN
 
@@ -396,11 +422,31 @@
             peak[n : n + 1] = new
 
     attend(lambda a: ins[a][...], step, True)
-    for d in range(1, places):
-
-        @pl.when(place + d < places)
-        def _(d=d):
-            remote(run, far.at[place], far_s.at[d], far_r.at[d], (place + d, tp)).start()
+    columns = jnp.transpose(facts)[:own_rows]
+
+    def group_of(names):
+        return jnp.floor((names + 0.5) / inner)
+
+    group = group_of(facts[heads : heads + 1, :own_rows])
+    ahead = lax.broadcasted_iota(jnp.int32, (own_rows, own_rows), 0)
+    ahead = ahead < lax.broadcasted_iota(jnp.int32, (own_rows, own_rows), 1)
+    same = jnp.logical_and(group_of(columns[:, heads : heads + 1]) == group, ahead)
+    placing = group * cap + jnp.sum(jnp.where(same, 1.0, 0.0), axis=0, keepdims=True)
+    slots = lax.broadcasted_iota(jnp.int32, (GROUPS * cap, own_rows), 0).astype(jnp.float32)
+    picker[...] = jnp.where(slots == placing, 1.0, 0.0).astype(jnp.bfloat16)
+    lane = lax.broadcasted_iota(jnp.int32, (own_rows, outgoing.shape[2] - features), 1)
+    extra = jnp.zeros(lane.shape, jnp.float32)
+    for e in range(inner):
+        weight = jnp.zeros((own_rows, 1), jnp.float32)
+        for k in range(picks):
+            name = columns[:, heads + k : heads + k + 1]
+            value = columns[:, heads + picks + k : heads + picks + k + 1]
+            weight = weight + jnp.where(name - inner * group_of(name) == e, value, 0.0)
+        top = weight.astype(jnp.bfloat16).astype(jnp.float32)
+        extra = jnp.where(lane == 2 * e, top, extra)
+        extra = jnp.where(lane == 2 * e + 1, weight - top, extra)
+    part = jnp.dot(picker[...], extra.astype(jnp.bfloat16), preferred_element_type=jnp.float32)
+    outgoing[:, :, features:] = part.astype(jnp.bfloat16).reshape(GROUPS, cap, lane.shape[1])
 
     for d in range(1, places):
 
@@ -426,7 +472,7 @@
                     def _(a=a):
                         lift(t, a).start()
 
-                cross(t, a).start()
+                pl.when(crosses(t, a))(lambda: cross(t, a).start())
 
     def own(t):
         @pl.when(o >= t)
@@ -434,131 +480,178 @@
             visit((o - t) * inner + i)
 
     def other(t):
+        slot = (o - t) * inner + far_i
+        for a in range(count):
+            where = blocks[a].at[slot]
+            if not detours(a):
+                pl.when((o >= t) if t > 0 else (far_i < i))(
+                    lambda: arrived(where, cross_r.at[t, a])
+                )
+                continue
+            if t > 0:
+                pl.when(o > t)(lambda: arrived(where, cross_r.at[t, a]))
+                pl.when(o == t)(lambda: arrived(where, turn_r.at[a]))
+            else:
+                pl.when(jnp.logical_or(far_i < i, o == 0))(
+                    lambda: arrived(where, cross_r.at[t, a])
+                )
+            if t < outer - 1:
+                pl.when(o == t)(lambda: detour(a).start())
+
         @pl.when((o >= t) if t > 0 else (far_i < i))
         def _():
-            slot = (o - t) * inner + far_i
-            for a in range(count):
-                arrived(blocks[a].at[slot], cross_r.at[t, a])
             visit(slot)
 
-    for t in range(outer):
-        if t > 0:
-            own(t)
-        if t + 1 < outer:
-            relay(t + 1)
-        other(t)
-
-    mixed = jnp.transpose(acc_w[...] / total[0:1]).astype(jnp.bfloat16)
-    att[:, :, :wide] = mixed.reshape(parts, own_rows, wide)
-    for n in range(1, heads):
-        piece = slice((n - 1) * HN, n * HN)
-        acc_n[piece] = acc_n[piece] / total[n : n + 1]
-    mixed = jnp.transpose(acc_n[...]).astype(jnp.bfloat16)
-    att[:, :, wide:] = mixed.reshape(parts, own_rows, narrow)
+    def finish():
+        mixed = jnp.transpose(acc_w[...] / total[0:1]).astype(jnp.bfloat16)
+        att[:, :, :wide] = mixed.reshape(parts, own_rows, wide)
+        for n in range(1, heads):
+            piece = slice((n - 1) * HN, n * HN)
+            acc_n[piece] = acc_n[piece] / total[n : n + 1]
+        mixed = jnp.transpose(acc_n[...]).astype(jnp.bfloat16)
+        att[:, :, wide:] = mixed.reshape(parts, own_rows, narrow)
+        for d in range(1, parts):
+            swap(d).start()
+        swapped[tp] = att[tp]
 
     def swap(d):
         k = (tp + d) % parts
         return remote(att.at[k], swapped.at[tp], swap_s.at[d], swap_r.at[d], (place, k))
 
-    for d in range(1, parts):
-        swap(d).start()
-    swapped[tp] = att[tp]
-    for t in range(outer):
-        for a in range(count):
-            if t < outer - 1:
-
-                @pl.when(jnp.logical_and(o >= t, o + 1 < outer))
-                def _(t=t, a=a):
-                    lift(t, a).wait_send()
-
-            @pl.when((o >= t) if t > 0 else (i < far_i))
-            def _(t=t, a=a):
-                cross(t, a).wait_send()
-
-    for d in range(1, places):
-
-        @pl.when(place + d < places)
-        def _(d=d):
-            remote(run, far.at[place], far_s.at[d], far_r.at[d], (place + d, tp)).wait_send()
-
-    loads[0].wait()
-    loads[1].wait()
-    for d in range(1, parts):
-        arrived(swapped.at[(tp - d + parts) % parts], swap_r.at[d])
-        swap(d).wait_send()
-    rows_w = jnp.concatenate([swapped[p, :, :wide] for p in range(parts)], axis=1)
-    rows_n = jnp.concatenate([swapped[p, :, wide:] for p in range(parts)], axis=1)
+    def settle():
+        for d in range(1, parts):
+            arrived(swapped.at[(tp - d + parts) % parts], swap_r.at[d])
+
     tile = math.gcd(features, 512)
-    squares = jnp.zeros((own_rows, 1), jnp.float32)
-    for n in range(features // tile):
-        at_n = pl.ds(n * tile, tile)
-        part = jnp.dot(rows_w, wide_w[:, at_n], preferred_element_type=jnp.float32)
-        part = part + jnp.dot(rows_n, narrow_w[:, at_n], preferred_element_type=jnp.float32)
-        part = (residual[:, at_n].astype(jnp.float32) + part).astype(jnp.bfloat16)
-        middle[:, at_n] = part
-        part = part.astype(jnp.float32)
-        squares = squares + jnp.sum(part * part, axis=1, keepdims=True)
-    factor = lax.rsqrt(squares / features + epsilon)
-    pick = picker[...]
-    for n in range(features // tile):
-        at_n = pl.ds(n * tile, tile)
-        part = middle[:, at_n].astype(jnp.float32) * factor * gain[:, at_n]
-        part = jnp.dot(pick, part.astype(jnp.bfloat16), preferred_element_type=jnp.float32)
-        outgoing[:, :, at_n] = part.astype(jnp.bfloat16).reshape(GROUPS, cap, tile)
-    part = jnp.dot(pick, extra[...], preferred_element_type=jnp.float32)
-    outgoing[:, :, features:] = part.astype(jnp.bfloat16).reshape(GROUPS, cap, extra.shape[1])
-
-    started = []
-
-    def push(kind, t, source, target, peer):
-        copy = remote(source, target, send.at[kind, t], take.at[kind, t], peer)
-        copy.start()
-        started.append(copy)
+
+    def project():
+        rows_w = jnp.concatenate([swapped[p, :, :wide] for p in range(parts)], axis=1)
+        rows_n = jnp.concatenate([swapped[p, :, wide:] for p in range(parts)], axis=1)
+        squares = jnp.zeros((own_rows, 1), jnp.float32)
+        for n in range(features // tile):
+            at_n = pl.ds(n * tile, tile)
+            part = jnp.dot(rows_w, wide_w[:, at_n], preferred_element_type=jnp.float32)
+            part = part + jnp.dot(rows_n, narrow_w[:, at_n], preferred_element_type=jnp.float32)
+            part = (residual[:, at_n].astype(jnp.float32) + part).astype(jnp.bfloat16)
+            middle[:, at_n] = part
+            part = part.astype(jnp.float32)
+            squares = squares + jnp.sum(part * part, axis=1, keepdims=True)
+        factor[...] = lax.rsqrt(squares / features + epsilon)
+
+    def ready():
+        for n in range(features // tile):
+            at_n = pl.ds(n * tile, tile)
+            part = middle[:, at_n].astype(jnp.float32) * factor[...] * gain[:, at_n]
+            part = jnp.dot(
+                picker[...], part.astype(jnp.bfloat16), preferred_element_type=jnp.float32
+            )
+            outgoing[:, :, at_n] = part.astype(jnp.bfloat16).reshape(GROUPS, cap, tile)
+
+    def route(kind, t):
+        mine, beside = pooled.at[t, c, i, y], pooled.at[t, c, far_i, y]
+        below, corners = pooled.at[t, c, i, far_y], pooled.at[t, c, far_i, far_y]
+        if kind == 0:
+            return outgoing.at[t, low], pooled.at[o, c, i, y, low], at(t, i, y, c)
+        if kind == 1:
+            return outgoing.at[t, high], pooled.at[o, c, i, y, high], at(t, i, y, c)
+        if kind == 2:
+            return mine.at[low], mine.at[low], across
+        if kind == 3:
+            return mine.at[high], mine.at[high], across
+        if kind == 4:
+            return mine.at[low], mine.at[low], along
+        if kind == 5:
+            return mine.at[high], mine.at[high], along
+        if kind == 6:
+            return beside.at[low], beside.at[low], along
+        if kind == 7:
+            return below.at[high], below.at[high], across
+        if kind in (8, 9, 10, 11):
+            slot = (mine, beside, below, corners)[kind - 8]
+            return slot, slot, mate
+        if kind == 12:
+            return answers.at[t, far_c], half.at[t], mate
+        if kind == 13:
+            return chip_a.at[t, far_i, far_y], from_x.at[t, far_y], across
+        if kind == 14:
+            return chip_a.at[t, far_i, y], from_x.at[t, y], across
+        if kind == 15:
+            return chip_b.at[t, far_y, far_i], from_y.at[t, far_i], along
+        if kind == 16:
+            return chip_b.at[t, far_y, i], from_y.at[t, i], along
+        if kind == 17:
+            return next_a.at[t], last_a.at[t], along
+        if kind == 18:
+            return next_b.at[t], last_b.at[t], across
+        return final.at[t], returned.at[o], at(t, i, y, c)
+
+    def copy_of(kind, t):
+        source, target, peer = route(kind, t)
+        mark = o if kind in (0, 1, 19) else t
+        return remote(source, target, send.at[kind, t], take.at[kind, mark], peer)
+
+    def push(kind, t):
+        if kind in (0, 1, 19):
+            pl.when(o != t)(lambda: copy_of(kind, t).start())
+        else:
+            copy_of(kind, t).start()
 
     def landed(kind, t, where):
         arrived(where, take.at[kind, t])
 
+    def late(t):
+        return jnp.logical_and(o + 2 <= t, o < outer - 2)
+
+    def send_rows(t):
+        push(0, t)
+        push(1, t)
+
+    def dispatch():
+        for t in range(outer):
+            pl.when(jnp.logical_not(late(t)))(lambda: send_rows(t))
+
+        pooled[o, c, i, y] = outgoing[o]
+
     def begin(t):
         slot = pooled.at[t, c, i, y]
-        source = outgoing.at[o]
-        if t > 0:
-            landed(0, t, slot)
-            source = slot
-        push(1, t, source, slot, across)
-        push(2, t, source, slot, along)
-        push(5, t, source, slot, mate)
-
-    def relay(t):
-        slot = pooled.at[t, c, far_i, y]
-        landed(1, t, slot)
-        part = pooled.at[t, c, far_i, y, low]
-        push(3, t, part, part, along)
-        push(6, t, slot, slot, mate)
-        slot = pooled.at[t, c, i, far_y]
-        landed(2, t, slot)
-        part = pooled.at[t, c, i, far_y, high]
-        push(4, t, part, part, across)
-        push(7, t, slot, slot, mate)
+
+        def hold(kind, part):
+            pl.when(o != t)(lambda: landed(kind, t, slot.at[part]))
+
+        hold(0, low)
+        push(2, t)
+        hold(1, high)
+        push(5, t)
+        push(3, t)
+        push(4, t)
+        push(8, t)
+
+    def pass_on(t):
+        beside, below = pooled.at[t, c, far_i, y], pooled.at[t, c, i, far_y]
+        landed(2, t, beside.at[low])
+        push(6, t)
+        landed(5, t, below.at[high])
+        push(7, t)
+        landed(3, t, beside.at[high])
+        push(9, t)
+        landed(4, t, below.at[low])
+        push(10, t)
 
     def corner(t):
-        landed(3, t, pooled.at[t, c, far_i, far_y, low])
-        landed(4, t, pooled.at[t, c, far_i, far_y, high])
-        slot = pooled.at[t, c, far_i, far_y]
-        push(8, t, slot, slot, mate)
+        landed(6, t, pooled.at[t, c, far_i, far_y, low])
+        landed(7, t, pooled.at[t, c, far_i, far_y, high])
+        push(11, t)
 
     def feed(t):
-        landed(5, t, pooled.at[t, far_c, i, y])
-        landed(6, t, pooled.at[t, far_c, far_i, y])
-        landed(7, t, pooled.at[t, far_c, i, far_y])
-        landed(8, t, pooled.at[t, far_c, far_i, far_y])
+        landed(8, t, pooled.at[t, far_c, i, y])
+        landed(9, t, pooled.at[t, far_c, far_i, y])
+        landed(10, t, pooled.at[t, far_c, i, far_y])
+        landed(11, t, pooled.at[t, far_c, far_i, far_y])
         rows = CORES * inner * ys * cap
         x = pooled[t, :, :, :, :, :features].reshape(rows, features)
         extra = pooled[t, :, :, :, :, features:].reshape(rows, -1).astype(jnp.float32)
         lane = lax.broadcasted_iota(jnp.int32, extra.shape, 1)
         scale = jnp.sum(jnp.where(lane // 2 == i, extra, 0.0), axis=1, keepdims=True)
-        if t == 0:
-            for copy in loads[2:]:
-                copy.wait()
         g = jnp.dot(x, gate[...], preferred_element_type=jnp.float32)
         u = jnp.dot(x, up[...], preferred_element_type=jnp.float32)
         hidden = (jax.nn.silu(g) * u).astype(jnp.bfloat16)
@@ -569,18 +662,20 @@
             answers[t, :, :, :, :, columns] = (
                 (part * scale).astype(jnp.bfloat16).reshape(CORES, inner, ys, cap, wide)
             )
-        push(9, t, answers.at[t, far_c], half.at[t], mate)
+        push(12, t)
 
     def gather(t):
-        landed(9, t, half.at[t])
+        landed(12, t, half.at[t])
         for i_ in range(inner):
             for y_ in range(ys):
                 total = answers[t, c, i_, y_].astype(jnp.float32)
                 total = (total + half[t, i_, y_].astype(jnp.float32)).astype(jnp.bfloat16)
                 chip_a[t, i_, y_] = total[:h]
                 chip_b[t, y_, i_] = total[h:]
-        push(10, t, chip_a.at[t, far_i], from_x.at[t], across)
-        push(11, t, chip_b.at[t, far_y], from_y.at[t], along)
+        push(13, t)
+        push(15, t)
+        push(14, t)
+        push(16, t)
 
     def add(*parts):
         total = parts[0].astype(jnp.float32)
@@ -589,49 +684,144 @@
         return total.astype(jnp.bfloat16)
 
     def turn(t):
-        landed(10, t, from_x.at[t])
+        landed(13, t, from_x.at[t, far_y])
         next_a[t] = add(chip_a[t, i, far_y], from_x[t, far_y])
-        push(12, t, next_a.at[t], last_a.at[t], along)
-        landed(11, t, from_y.at[t])
+        push(17, t)
+        landed(15, t, from_y.at[t, far_i])
         next_b[t] = add(chip_b[t, y, far_i], from_y[t, far_i])
-        push(13, t, next_b.at[t], last_b.at[t], across)
+        push(18, t)
 
     def home(t):
-        landed(12, t, last_a.at[t])
-        landed(13, t, last_b.at[t])
-        target = returned.at[o] if t == 0 else final.at[t]
-        target[:h] = add(chip_a[t, i, y], from_x[t, y], last_a[t])
-        target[h:] = add(chip_b[t, y, i], from_y[t, i], last_b[t])
-        if t > 0:
-            push(14, t, final.at[t], returned.at[o], at((o - t + outer) % outer, i, y, c))
-
-    for d in range(1, outer):
-        there = (o + d) % outer
-        push(0, d, outgoing.at[there], pooled.at[d, c, i, y], at(there, i, y, c))
-    pooled[0, c, i, y] = outgoing[o]
-    begin(0)
-    begin(1)
-    for k in range(outer + 3):
-        if k < outer:
-            relay(k)
-            if k + 2 < outer:
-                begin(k + 2)
+        landed(14, t, from_x.at[t, y])
+        landed(16, t, from_y.at[t, i])
+        landed(17, t, last_a.at[t])
+        landed(18, t, last_b.at[t])
+        final[t, :h] = add(chip_a[t, i, y], from_x[t, y], last_a[t])
+        final[t, h:] = add(chip_b[t, y, i], from_y[t, i], last_b[t])
+        push(19, t)
+
+    final_plane = o == outer - 1
+    relay(1)
+    other(0)
+    own(1)
+    relay(2)
+    other(1)
+    own(2)
+    relay(3)
+    other(2)
+    own(3)
+
+    other(3)
+    finish()
+
+    loads[0].wait()
+    loads[1].wait()
+    settle()
+
+    project()
+    ready()
+    dispatch()
+    for copy in loads[2:]:
+        copy.wait()
+
+    @pl.when(final_plane)
+    def _():
+        begin(0)
+        begin(1)
+        pass_on(0)
+        begin(2)
+        begin(3)
+        corner(0)
+        feed(0)
+        pass_on(1)
+        corner(1)
+        feed(1)
+        gather(0)
+        pass_on(2)
+        gather(1)
+        pass_on(3)
+        corner(2)
+        feed(2)
+        turn(0)
+        gather(2)
+        corner(3)
+        feed(3)
+        turn(1)
+        gather(3)
+        home(0)
+        turn(2)
+        home(1)
+        turn(3)
+        home(2)
+        home(3)
+
+    @pl.when(jnp.logical_not(final_plane))
+    def _():
+        begin(0)
+        pass_on(0)
+        for t in range(outer):
+            pl.when(late(t))(lambda: send_rows(t))
+        for k in range(outer):
+            if k + 1 < outer:
+                begin(k + 1)
+            if k >= 2:
+                home(k - 2)
             corner(k)
-        if 0 <= k - 1 < outer:
-            gather(k - 1)
-        if k < outer:
             feed(k)
-        if 0 <= k - 3 < outer:
-            home(k - 3)
-        if 0 <= k - 2 < outer:
-            turn(k - 2)
-    for t in range(1, outer):
-        landed(14, t, returned.at[(o + t) % outer])
-    for copy in started:
-        copy.wait_send()
+            if k + 1 < outer:
+                pass_on(k + 1)
+            if k >= 1:
+                turn(k - 1)
+            gather(k)
+        home(outer - 2)
+        turn(outer - 1)
+        home(outer - 1)
+
+    for t in range(outer):
+        for a in range(count):
+            if t < outer - 1:
+
+                @pl.when(jnp.logical_and(o >= t, o + 1 < outer))
+                def _(t=t, a=a):
+                    lift(t, a).wait_send()
+
+            @pl.when(crosses(t, a))
+            def _(t=t, a=a):
+                cross(t, a).wait_send()
+
+    for a in range(count):
+        if detours(a):
+
+            @pl.when(o + 1 < outer)
+            def _(a=a):
+                detour(a).wait_send()
+
+    for d in range(1, places):
+
+        @pl.when(place + d < places)
+        def _(d=d):
+            remote(run, far.at[place], far_s.at[d], far_r.at[d], (place + d, tp)).wait_send()
+
+    for d in range(1, parts):
+        swap(d).wait_send()
+
+    returned[o] = final[o]
+    for t in range(outer):
+
+        @pl.when(o != t)
+        def _(t=t):
+            landed(19, t, returned.at[t])
+
+    for t in range(outer):
+        for kind in range(20):
+            if kind in (0, 1, 19):
+                pl.when(o != t)(lambda: copy_of(kind, t).wait_send())
+            else:
+                copy_of(kind, t).wait_send()
+
     slots = returned[...].reshape(GROUPS * cap, features)
     combined = lax.dot_general(
-        pick, slots, (((0,), (0,)), ((), ())), preferred_element_type=jnp.float32
+        picker[...], slots, (((0,), (0,)), ((), ())), preferred_element_type=jnp.float32
     )
     result[...] = (middle[...].astype(jnp.float32) + combined).astype(jnp.bfloat16)
 
@@ -661,33 +851,13 @@
     parts = lax.axis_size("tp")
     ys = parts // CORES
     own_rows, features = residual.shape
-    gates = jnp.concatenate([gate_wide, gate_narrow], axis=1).T
-    gates = jnp.pad(gates, ((0, -gates.shape[0] % 8), (0, 0)))
     rows, wide = query_wide.shape
     narrow = query_narrow.shape[1]
-
+    heads = gate_wide.shape[1] + gate_narrow.shape[1]
+    lines = pl.cdiv(heads + 2 * inner, 8) * 8
     cap = own_rows * GROUPS // places
-    group = routing[:, 0] // inner
-    matches = (group[:, None] == jnp.arange(GROUPS, dtype=jnp.int32)[None, :]).astype(jnp.int32)
-    ranking = jnp.sum((jnp.cumsum(matches, axis=0) - matches) * matches, axis=1)
-    placing = group * cap + ranking
-    picker = placing[None, :] == jnp.arange(GROUPS * cap, dtype=jnp.int32)[:, None]
-    picker = picker.astype(jnp.bfloat16)
-    of_expert = jnp.sum(
-        jnp.where(
-            (routing % inner)[:, :, None] == jnp.arange(inner, dtype=jnp.int32)[None, None, :],
-            route_weight[:, :, None],
-            0.0,
-        ),
-        axis=1,
-    )
-    high = of_expert.astype(jnp.bfloat16)
-    rest = (of_expert - high.astype(jnp.float32)).astype(jnp.bfloat16)
-    extra = jnp.stack([high, rest], axis=2).reshape(own_rows, 2 * inner)
-    extra = jnp.pad(extra, ((0, 0), (0, -2 * inner % 128)))
-
     h = cap // 2
-    width = features + extra.shape[1]
+    width = features + 128 * pl.cdiv(2 * inner, 128)
     kind, full = jnp.bfloat16, jnp.float32
 
     def vmem(*shape, dtype=kind):
@@ -698,10 +868,10 @@
         vmem(places, rows, wide),
         vmem(places, rows, narrow),
         vmem(places, rows, narrow),
-        vmem(places, gates.shape[0], rows, dtype=full),
-        vmem(gates.shape[0], rows, dtype=full),
-        vmem(gates.shape[0], rows, dtype=full),
-        vmem(gates.shape[0], rows, dtype=full),
+        vmem(places, lines, rows, dtype=full),
+        vmem(lines, rows, dtype=full),
+        vmem(lines, rows, dtype=full),
+        vmem(lines, rows, dtype=full),
         vmem(wide, rows, dtype=full),
         vmem(narrow, rows, dtype=full),
         vmem(parts, own_rows, wide + narrow),
@@ -726,30 +896,38 @@
         vmem(outer, h, features),
         vmem(outer, h, features),
         vmem(outer, cap, features),
+        vmem(GROUPS * cap, own_rows),
+        vmem(lines, rows, dtype=full),
+        vmem(own_rows, 1, dtype=full),
         DMA((5,)),
         DMA((outer, 4)),
         DMA((outer, 4)),
         DMA((outer, 4)),
         DMA((outer, 4)),
+        DMA((4,)),
+        DMA((4,)),
         DMA((places,)),
         DMA((places,)),
         DMA((parts,)),
         DMA((parts,)),
-        DMA((15, outer)),
-        DMA((15, outer)),
+        DMA((20, outer)),
+        DMA((20, outer)),
     ]
     anywhere = pl.BlockSpec(memory_space=pl.ANY)
     return pl.pallas_call(
         functools.partial(layer_kernel, outer, inner, ys),
         out_shape=jax.ShapeDtypeStruct(residual.shape, residual.dtype),
-        in_specs=[VMEM] * 11 + [anywhere] * 5,
+        in_specs=[VMEM] * 12 + [anywhere] * 5,
         out_specs=VMEM,
         scratch_shapes=scratch,
         compiler_params=pltpu.CompilerParams(
             collective_id=1, has_side_effects=True, vmem_limit_bytes=56 * 1024 * 1024
         ),
     )(
-        gates,
+        gate_wide.T,
+        gate_narrow.T,
+        routing.T,
+        route_weight.T,
         query_wide,
         key_wide,
         value_wide,
@@ -758,8 +936,6 @@
         value_narrow,
         residual,
         norm_gain[None, :],
-        picker,
-        extra,
         out_wide,
         out_narrow,
         gate_weight,

time: 101 us -> 82.6 us (0.82)
  Pallas kernels: 92.8 us -> 80.6 us
  other arithmetic: 4.46 us -> 0 us
  local copies, waits for them, and re-layouts: 3 us -> 1.67 us
    pallas_call x1, Pallas kernels: 92.8 us -> 80.6 us  [fast_body(): pl.pallas_call(functools.partial(layer_kernel, outer, inner, ys), out_sha...]
    pad x2 -> x0, local copies, waits for them, and re-layouts: 1.21 us -> none  [the longest x1 0.61 us: fast_body(): extra = jnp.pad(extra, ((0, 0), (0, -2 * inner % 128)))]
where the time goes in v3:
time: 82.6 us; the launch traced here: 82.3 us
  Pallas kernels  80.6 us (98%)
  local copies, waits for them, and re-layouts  1.67 us (2%)
    pallas_call x1, Pallas kernels, fast_body(): pl.pallas_call(functools.partial(layer_kernel, outer, inner, ys), out_sha...  80.6 us
    unnamed x1, local copies, waits for them, and re-layouts  1.67 us

profile of v3, /device:TPU:16, one launch (start us, length us, event | category | flops | bytes accessed | tf_op | source)
XLA Modules:
  0.0 82.3 jit_solution(12089240599267740977)
XLA Ops:
  0.0 80.6 %shard_map.163 = bf16[64,2048]{1,0:T(8,128)(2,1)} custom-call(f32[1,256]{1,0:T(1,128)} %bitcast.7, f32[2,256]{1,0:T(2,128)} %bitcast.6, s32[2,64]{1,0:T(2,128)} %bitcast.8, f32[2,64]{1,0:T(2,128)} %bitcast.9, bf16[256,128]{1,0:T(8,128)(2,1)} %refs_4_.1, bf16[256,128]{1,0:T(8,128)(2,1)} %refs_5_.1, bf16[256,128]{1,0:T(8,128)(2,1)} %refs_6_.1, ...), custom_call_target="tpu_custom_call" | custom-call | tf_op jit(solution)/shard_map/pallas_call | solution.py:917
  80.6 1.7 %copy.19 = bf16[64,2048]{1,0:T(8,128)(2,1)} copy(bf16[64,2048]{1,0:T(8,128)(2,1)} %shard_map.163) | data formatting | bytes 524288

commit v4 on v3

--- a/solution.py
+++ b/solution.py
@@ -268,6 +268,10 @@
 DMA = pltpu.SemaphoreType.DMA
 
 
+SENDS = [0, 1, 2, 3, 4, 5, 6, 7, 8, 8, 8, 8, 9, 10, 10, 10, 10, 10, 10, 11, 12, 9, 10]
+TAKES = [0, 1, 2, 3, 4, 5, 6, 6, 7, 7, 7, 7, 8, 9, 11, 10, 11, 11, 11, 12, 8, 9, 10]
+
+
 LOG2E = math.log2(math.e)
 
 
@@ -279,8 +283,9 @@
     wide_w, narrow_w, gate, up, down, middle, outgoing, returned = refs[27:35]
     pooled, answers, half, chip_a, chip_b, from_x, from_y, next_a, next_b = refs[35:44]
     last_a, last_b, final, picker, board, factor = refs[44:50]
-    load, lift_s, lift_r, cross_s, cross_r, turn_s, turn_r = refs[50:57]
-    far_s, far_r, swap_s, swap_r, send, take = refs[57:]
+    hidden, hidden_in, parts_own, parts_in, both, from_both, ended = refs[50:57]
+    load, lift_s, lift_r, cross_s, cross_r, turn_s, turn_r = refs[57:64]
+    far_s, far_r, swap_s, swap_r, give_s, give_r, send, take = refs[64:]
     place, tp = lax.axis_index("sp"), lax.axis_index("tp")
     o, i, y, c = place // inner, place % inner, tp // CORES, tp % CORES
     far_i, far_y, far_c = (i + 1) % inner, (y + 1) % ys, (c + 1) % CORES
@@ -292,7 +297,9 @@
     cap = outgoing.shape[1]
     h = cap // 2
     low, high = pl.ds(0, h), pl.ds(h, h)
-
+    units = gate.shape[1]
+    deep = o >= outer - 2
+    final_plane = o == outer - 1
     def at(o_, i_, y_, c_):
         return (o_ * inner + i_, y_ * CORES + c_)
 
@@ -306,7 +313,7 @@
                 (out_narrow, narrow_w),
                 (gate_hbm.at[0], gate),
                 (up_hbm.at[0], up),
-                (down_hbm.at[0], down),
+                (down_hbm.at[0], down.at[y]),
             ]
         )
     ]
@@ -350,22 +357,30 @@
     def lift(t, a):
         source, target = source_of(t, a)
         return remote(
-            source, target, lift_s.at[t, a], lift_r.at[t, a], at(o + 1, i, y, c)
+            source, target, lift_s.at[t, a // 2], lift_r.at[t, a // 2], at(o + 1, i, y, c)
         )
 
     def cross(t, a):
         source, target = source_of(t, a)
-        return remote(source, target, cross_s.at[t, a], cross_r.at[t, a], across)
+        return remote(source, target, cross_s.at[t, a // 2], cross_r.at[t, a // 2], across)
+
+    def twin(p):
+        return blocks[2 * p].at[pl.ds(0, 2)]
 
     def arrived(where, semaphore):
         remote(where, where, semaphore, semaphore, mate).wait_recv()
 
     def detour(a):
         slot = blocks[a].at[far_i]
-        return remote(slot, slot, turn_s.at[a], turn_r.at[a], at(o + 1, i, y, c))
+        return remote(slot, slot, turn_s.at[0], turn_r.at[0], at(o + 1, i, y, c))
 
     def detours(a):
         return a >= count // 2
+
+    def give(p):
+        lines = pl.ds(p * units // outer, units // outer)
+        target = down.at[y, lines]
+        return remote(down_hbm.at[0, lines], target, give_s.at[0], give_r.at[0], along)
 
     def crosses(t, a):
         if t == 0:
@@ -381,6 +396,9 @@
         @pl.when(crosses(0, a))
         def _(a=a):
             cross(0, a).start()
+
+    for p in range(outer):
+        pl.when(deep if p < outer - 1 else final_plane)(lambda: give(p).start())
 
     head_lane = lax.broadcasted_iota(jnp.int32, (rows, narrow), 1) // HN
 
@@ -464,15 +482,12 @@
     def relay(t):
         @pl.when(o >= t)
         def _():
-            for a in range(count):
-                arrived(blocks[a].at[(o - t) * inner + i], lift_r.at[t - 1, a])
-                if t < outer - 1:
-
-                    @pl.when(o + 1 < outer)
-                    def _(a=a):
-                        lift(t, a).start()
-
-                pl.when(crosses(t, a))(lambda: cross(t, a).start())
+            for p in range(count // 2):
+                arrived(twin(p), lift_r.at[t - 1, p])
+                for a in (2 * p, 2 * p + 1):
+                    if t < outer - 1:
+                        pl.when(o + 1 < outer)(lambda: lift(t, a).start())
+                    pl.when(crosses(t, a))(lambda: cross(t, a).start())
 
     def own(t):
         @pl.when(o >= t)
@@ -481,21 +496,15 @@
 
     def other(t):
         slot = (o - t) * inner + far_i
-        for a in range(count):
-            where = blocks[a].at[slot]
-            if not detours(a):
-                pl.when((o >= t) if t > 0 else (far_i < i))(
-                    lambda: arrived(where, cross_r.at[t, a])
-                )
-                continue
-            if t > 0:
-                pl.when(o > t)(lambda: arrived(where, cross_r.at[t, a]))
-                pl.when(o == t)(lambda: arrived(where, turn_r.at[a]))
-            else:
-                pl.when(jnp.logical_or(far_i < i, o == 0))(
-                    lambda: arrived(where, cross_r.at[t, a])
-                )
-            if t < outer - 1:
+        needed = (o >= t) if t > 0 else (far_i < i)
+        pl.when(needed)(lambda: arrived(twin(0), cross_r.at[t, 0]))
+        if t > 0:
+            pl.when(o > t)(lambda: arrived(twin(1), cross_r.at[t, 1]))
+            pl.when(o == t)(lambda: arrived(twin(1), turn_r.at[0]))
+        else:
+            pl.when(jnp.logical_or(needed, o == 0))(lambda: arrived(twin(1), cross_r.at[t, 1]))
+        if t < outer - 1:
+            for a in range(count // 2, count):
                 pl.when(o == t)(lambda: detour(a).start())
 
         @pl.when((o >= t) if t > 0 else (far_i < i))
@@ -516,11 +525,10 @@
 
     def swap(d):
         k = (tp + d) % parts
-        return remote(att.at[k], swapped.at[tp], swap_s.at[d], swap_r.at[d], (place, k))
+        return remote(att.at[k], swapped.at[tp], swap_s.at[0], swap_r.at[0], (place, k))
 
     def settle():
-        for d in range(1, parts):
-            arrived(swapped.at[(tp - d + parts) % parts], swap_r.at[d])
+        arrived(swapped.at[pl.ds(0, parts - 1)], swap_r.at[0])
 
     tile = math.gcd(features, 512)
 
@@ -583,12 +591,18 @@
             return next_a.at[t], last_a.at[t], along
         if kind == 18:
             return next_b.at[t], last_b.at[t], across
+        if kind == 20:
+            return hidden.at[t, far_y], hidden_in.at[t], along
+        if kind == 21:
+            return parts_own.at[t, far_c], parts_in.at[t], mate
+        if kind == 22:
+            return both.at[t, far_i], from_both.at[t], across
         return final.at[t], returned.at[o], at(t, i, y, c)
 
     def copy_of(kind, t):
         source, target, peer = route(kind, t)
         mark = o if kind in (0, 1, 19) else t
-        return remote(source, target, send.at[kind, t], take.at[kind, mark], peer)
+        return remote(source, target, send.at[SENDS[kind]], take.at[TAKES[kind], mark], peer)
 
     def push(kind, t):
         if kind in (0, 1, 19):
@@ -597,7 +611,7 @@
             copy_of(kind, t).start()
 
     def landed(kind, t, where):
-        arrived(where, take.at[kind, t])
+        arrived(where, take.at[TAKES[kind], t])
 
     def late(t):
         return jnp.logical_and(o + 2 <= t, o < outer - 2)
@@ -607,7 +621,7 @@
         push(1, t)
 
     def dispatch():
-        for t in range(outer):
+        for t in reversed(range(outer)):
             pl.when(jnp.logical_not(late(t)))(lambda: send_rows(t))
 
         pooled[o, c, i, y] = outgoing[o]
@@ -638,15 +652,11 @@
         push(10, t)
 
     def corner(t):
-        landed(6, t, pooled.at[t, c, far_i, far_y, low])
-        landed(7, t, pooled.at[t, c, far_i, far_y, high])
+        landed(6, t, pooled.at[t, c, far_i, far_y])
         push(11, t)
 
     def feed(t):
-        landed(8, t, pooled.at[t, far_c, i, y])
-        landed(9, t, pooled.at[t, far_c, far_i, y])
-        landed(10, t, pooled.at[t, far_c, i, far_y])
-        landed(11, t, pooled.at[t, far_c, far_i, far_y])
+        landed(8, t, pooled.at[t, far_c])
         rows = CORES * inner * ys * cap
         x = pooled[t, :, :, :, :, :features].reshape(rows, features)
         extra = pooled[t, :, :, :, :, features:].reshape(rows, -1).astype(jnp.float32)
@@ -654,11 +664,11 @@
         scale = jnp.sum(jnp.where(lane // 2 == i, extra, 0.0), axis=1, keepdims=True)
         g = jnp.dot(x, gate[...], preferred_element_type=jnp.float32)
         u = jnp.dot(x, up[...], preferred_element_type=jnp.float32)
-        hidden = (jax.nn.silu(g) * u).astype(jnp.bfloat16)
+        made = (jax.nn.silu(g) * u).astype(jnp.bfloat16)
         wide = math.gcd(features, 512)
         for n in range(features // wide):
             columns = pl.ds(n * wide, wide)
-            part = jnp.dot(hidden, down[:, columns], preferred_element_type=jnp.float32)
+            part = jnp.dot(made, down[y, :, columns], preferred_element_type=jnp.float32)
             answers[t, :, :, :, :, columns] = (
                 (part * scale).astype(jnp.bfloat16).reshape(CORES, inner, ys, cap, wide)
             )
@@ -692,15 +702,52 @@
         push(18, t)
 
     def home(t):
-        landed(14, t, from_x.at[t, y])
-        landed(16, t, from_y.at[t, i])
-        landed(17, t, last_a.at[t])
-        landed(18, t, last_b.at[t])
+        landed(14, t, chip_a.at[t])
         final[t, :h] = add(chip_a[t, i, y], from_x[t, y], last_a[t])
         final[t, h:] = add(chip_b[t, y, i], from_y[t, i], last_b[t])
         push(19, t)
 
-    final_plane = o == outer - 1
+    def enter(t):
+        landed(8, t, pooled.at[t, far_c])
+        x = pooled[t, :, :, :, :, :features].reshape(CORES * inner * ys * cap, features)
+        g = jnp.dot(x, gate[...], preferred_element_type=jnp.float32)
+        u = jnp.dot(x, up[...], preferred_element_type=jnp.float32)
+        made = (jax.nn.silu(g) * u).astype(jnp.bfloat16)
+        made = made.reshape(CORES, inner, ys, cap, units)
+        for y_ in range(ys):
+            hidden[t, y_] = made[:, :, y_]
+        push(20, t)
+
+    def complete():
+        arrived(down.at[far_y], give_r.at[0])
+
+    def mix(t):
+        landed(20, t, hidden_in.at[t])
+        lines = CORES * inner * cap
+        extra = pooled[t, :, :, y, :, features:].reshape(lines, -1).astype(jnp.float32)
+        lane = lax.broadcasted_iota(jnp.int32, extra.shape, 1)
+        scale = jnp.sum(jnp.where(lane // 2 == i, extra, 0.0), axis=1, keepdims=True)
+        mine = hidden[t, y].reshape(lines, units)
+        theirs = hidden_in[t].reshape(lines, units)
+        for n in range(features // tile):
+            at_n = pl.ds(n * tile, tile)
+            part = jnp.dot(mine, down[y, :, at_n], preferred_element_type=jnp.float32)
+            part = part + jnp.dot(theirs, down[far_y, :, at_n], preferred_element_type=jnp.float32)
+            parts_own[t, :, :, :, at_n] = (
+                (part * scale).astype(jnp.bfloat16).reshape(CORES, inner, cap, tile)
+            )
+        push(21, t)
+
+    def pair(t):
+        landed(21, t, parts_in.at[t])
+        both[t] = add(parts_own[t, c], parts_in[t])
+        push(22, t)
+
+    def leave(t):
+        landed(22, t, from_both.at[t])
+        final[t] = add(both[t, i], from_both[t])
+        push(19, t)
+
     relay(1)
     other(0)
     own(1)
@@ -717,84 +764,92 @@
     loads[0].wait()
     loads[1].wait()
     settle()
-
+    pl.when(o == outer - 2)(lambda: give(outer - 1).start())
     project()
     ready()
     dispatch()
     for copy in loads[2:]:
         copy.wait()
 
-    @pl.when(final_plane)
+    @pl.when(deep)
     def _():
         begin(0)
         begin(1)
         pass_on(0)
         begin(2)
         begin(3)
+        pass_on(1)
         corner(0)
-        feed(0)
-        pass_on(1)
+        enter(0)
+        complete()
+        pass_on(2)
         corner(1)
-        feed(1)
-        gather(0)
-        pass_on(2)
-        gather(1)
+        mix(0)
+        enter(1)
         pass_on(3)
+        pair(0)
         corner(2)
-        feed(2)
-        turn(0)
-        gather(2)
+        enter(2)
+        mix(1)
+        pair(1)
         corner(3)
-        feed(3)
-        turn(1)
-        gather(3)
-        home(0)
-        turn(2)
-        home(1)
-        turn(3)
-        home(2)
-        home(3)
-
-    @pl.when(jnp.logical_not(final_plane))
+        mix(2)
+        enter(3)
+        leave(0)
+        pair(2)
+        mix(3)
+        leave(1)
+        pair(3)
+        leave(2)
+        leave(3)
+
+    @pl.when(jnp.logical_not(deep))
     def _():
         begin(0)
         pass_on(0)
         for t in range(outer):
             pl.when(late(t))(lambda: send_rows(t))
-        for k in range(outer):
-            if k + 1 < outer:
-                begin(k + 1)
-            if k >= 2:
-                home(k - 2)
-            corner(k)
-            feed(k)
-            if k + 1 < outer:
-                pass_on(k + 1)
-            if k >= 1:
-                turn(k - 1)
-            gather(k)
-        home(outer - 2)
-        turn(outer - 1)
-        home(outer - 1)
+        begin(1)
+        corner(0)
+        feed(0)
+        pass_on(1)
+        gather(0)
+        begin(2)
+        corner(1)
+        feed(1)
+        pass_on(2)
+        turn(0)
+        gather(1)
+        begin(3)
+        home(0)
+        corner(2)
+        feed(2)
+        pass_on(3)
+        turn(1)
+        gather(2)
+        home(1)
+        corner(3)
+        feed(3)
+        turn(2)
+        gather(3)
+        home(2)
+        turn(3)
+        home(3)
+
+    @pl.when(deep)
+    def _():
+        remote(down.at[y], down.at[y], give_s.at[0], give_r.at[0], mate).wait_send()
+
+    def sent(p, semaphore):
+        remote(twin(p), twin(p), semaphore, semaphore, mate).wait_send()
 
     for t in range(outer):
-        for a in range(count):
+        for p in range(count // 2):
             if t < outer - 1:
-
-                @pl.when(jnp.logical_and(o >= t, o + 1 < outer))
-                def _(t=t, a=a):
-                    lift(t, a).wait_send()
-
-            @pl.when(crosses(t, a))
-            def _(t=t, a=a):
-                cross(t, a).wait_send()
-
-    for a in range(count):
-        if detours(a):
-
-            @pl.when(o + 1 < outer)
-            def _(a=a):
-                detour(a).wait_send()
+                pl.when(jnp.logical_and(o >= t, o + 1 < outer))(lambda: sent(p, lift_s.at[t, p]))
+            pl.when(crosses(t, 2 * p))(lambda: sent(p, cross_s.at[t, p]))
+
+    pl.when(o + 1 < outer)(lambda: sent(1, turn_s.at[0]))
 
     for d in range(1, places):
 
@@ -802,28 +857,52 @@
         def _(d=d):
             remote(run, far.at[place], far_s.at[d], far_r.at[d], (place + d, tp)).wait_send()
 
-    for d in range(1, parts):
-        swap(d).wait_send()
+    others = att.at[pl.ds(0, parts - 1)]
+    remote(others, others, swap_s.at[0], swap_r.at[0], mate).wait_send()
+
+    def returns(t):
+        pl.when(o != t)(lambda: landed(19, t, returned.at[t]))
 
     returned[o] = final[o]
     for t in range(outer):
-
-        @pl.when(o != t)
-        def _(t=t):
-            landed(19, t, returned.at[t])
-
-    for t in range(outer):
-        for kind in range(20):
-            if kind in (0, 1, 19):
-                pl.when(o != t)(lambda: copy_of(kind, t).wait_send())
-            else:
-                copy_of(kind, t).wait_send()
-
-    slots = returned[...].reshape(GROUPS * cap, features)
-    combined = lax.dot_general(
-        picker[...], slots, (((0,), (0,)), ((), ())), preferred_element_type=jnp.float32
-    )
-    result[...] = (middle[...].astype(jnp.float32) + combined).astype(jnp.bfloat16)
+        returns(t)
+
+    def drain(kind, whole):
+        remote(whole, whole, send.at[SENDS[kind]], send.at[SENDS[kind]], mate).wait_send()
+
+    drain(0, outgoing.at[pl.ds(0, outer - 1), low])
+    drain(1, outgoing.at[pl.ds(0, outer - 1), high])
+    for kind in range(2, 8):
+        drain(kind, pooled.at[:, 0, 0, 0, low if kind in (2, 4, 6) else high])
+    drain(8, pooled.at[pl.ds(0, outer // 2)])
+    drain(19, final.at[pl.ds(0, outer - 1)])
+
+    @pl.when(deep)
+    def _():
+        drain(20, hidden_in)
+        drain(21, parts_in)
+        drain(22, from_both)
+
+    @pl.when(jnp.logical_not(deep))
+    def _():
+        drain(12, half)
+        drain(13, half.at[pl.ds(0, 3 * outer // 4)])
+
+    def combine():
+        copies = []
+        for n in range(features // tile):
+            at_n = pl.ds(n * tile, tile)
+            slots = returned[:, :, at_n].reshape(GROUPS * cap, tile)
+            combined = lax.dot_general(
+                picker[...], slots, (((0,), (0,)), ((), ())), preferred_element_type=jnp.float32
+            )
+            ended[n] = (middle[:, at_n].astype(jnp.float32) + combined).astype(jnp.bfloat16)
+            copies.append(pltpu.make_async_copy(ended.at[n], result.at[:, at_n], load.at[5 + n]))
+            copies[-1].start()
+        for copy in copies:
+            copy.wait()
+
+    combine()
 
 
 def fast_body(
@@ -857,6 +936,8 @@
     lines = pl.cdiv(heads + 2 * inner, 8) * 8
     cap = own_rows * GROUPS // places
     h = cap // 2
+    units = down_weight.shape[1]
+    tiles = features // math.gcd(features, 512)
     width = features + 128 * pl.cdiv(2 * inner, 128)
     kind, full = jnp.bfloat16, jnp.float32
 
@@ -880,7 +961,7 @@
         vmem(*out_narrow.shape),
         vmem(*gate_weight.shape[1:]),
         vmem(*up_weight.shape[1:]),
-        vmem(*down_weight.shape[1:]),
+        vmem(ys, units, features),
         vmem(own_rows, features),
         vmem(GROUPS, cap, width),
         vmem(outer, cap, features),
@@ -899,26 +980,35 @@
         vmem(GROUPS * cap, own_rows),
         vmem(lines, rows, dtype=full),
         vmem(own_rows, 1, dtype=full),
-        DMA((5,)),
-        DMA((outer, 4)),
-        DMA((outer, 4)),
-        DMA((outer, 4)),
-        DMA((outer, 4)),
-        DMA((4,)),
-        DMA((4,)),
+        vmem(outer, ys, CORES, inner, cap, units),
+        vmem(outer, CORES, inner, cap, units),
+        vmem(outer, CORES, inner, cap, features),
+        vmem(outer, inner, cap, features),
+        vmem(outer, inner, cap, features),
+        vmem(outer, cap, features),
+        vmem(tiles, own_rows, features // tiles),
+        DMA((5 + tiles,)),
+        DMA((outer - 1, 2)),
+        DMA((outer - 1, 2)),
+        DMA((outer, 2)),
+        DMA((outer, 2)),
+        DMA((1,)),
+        DMA((1,)),
         DMA((places,)),
         DMA((places,)),
-        DMA((parts,)),
-        DMA((parts,)),
-        DMA((20, outer)),
-        DMA((20, outer)),
+        DMA((1,)),
+        DMA((1,)),
+        DMA((1,)),
+        DMA((1,)),
+        DMA((1 + max(SENDS),)),
+        DMA((1 + max(TAKES), outer)),
     ]
     anywhere = pl.BlockSpec(memory_space=pl.ANY)
     return pl.pallas_call(
         functools.partial(layer_kernel, outer, inner, ys),
         out_shape=jax.ShapeDtypeStruct(residual.shape, residual.dtype),
         in_specs=[VMEM] * 12 + [anywhere] * 5,
-        out_specs=VMEM,
+        out_specs=anywhere,
         scratch_shapes=scratch,
         compiler_params=pltpu.CompilerParams(
             collective_id=1, has_side_effects=True, vmem_limit_bytes=56 * 1024 * 1024

time: 82.6 us -> 79.1 us (0.958); the launches traced: 82.3 us -> 77.8 us
  Pallas kernels: 80.6 us -> 76.1 us
    pallas_call x1, Pallas kernels: 80.6 us -> 76.1 us  [fast_body(): pl.pallas_call(functools.partial(layer_kernel, outer, inner, ys), out_sha...]
where the time goes in v4:
time: 79.1 us; the launch traced here: 77.8 us
  Pallas kernels  76.1 us (96%)
  local copies, waits for them, and re-layouts  1.67 us (2%)
    pallas_call x1, Pallas kernels, fast_body(): pl.pallas_call(functools.partial(layer_kernel, outer, inner, ys), out_sha...  76.1 us
    unnamed x1, local copies, waits for them, and re-layouts  1.67 us

profile of v4, /device:TPU:16, one launch (start us, length us, event | category | flops | bytes accessed | tf_op | source)
XLA Modules:
  0.0 77.8 jit_solution(10979443622807378866)
XLA Ops:
  0.0 76.1 %shard_map.163 = bf16[64,2048]{1,0:T(8,128)(2,1)} custom-call(f32[1,256]{1,0:T(1,128)} %bitcast.7, f32[2,256]{1,0:T(2,128)} %bitcast.6, s32[2,64]{1,0:T(2,128)} %bitcast.8, f32[2,64]{1,0:T(2,128)} %bitcast.9, bf16[256,128]{1,0:T(8,128)(2,1)} %refs_4_.1, bf16[256,128]{1,0:T(8,128)(2,1)} %refs_5_.1, bf16[256,128]{1,0:T(8,128)(2,1)} %refs_6_.1, ...), custom_call_target="tpu_custom_call" | custom-call | tf_op jit(solution)/shard_map/pallas_call | solution.py:1007
  76.1 1.7 %copy.19 = bf16[64,2048]{1,0:T(8,128)(2,1)} copy(bf16[64,2048]{1,0:T(8,128)(2,1)} %shard_map.163) | data formatting | bytes 524288

commit v5 on v4

--- a/solution.py
+++ b/solution.py
@@ -357,7 +357,7 @@
     def lift(t, a):
         source, target = source_of(t, a)
         return remote(
-            source, target, lift_s.at[t, a // 2], lift_r.at[t, a // 2], at(o + 1, i, y, c)
+            source, target, lift_s.at[t, a // 2], lift_r.at[t, a], at(o + 1, i, y, c)
         )
 
     def cross(t, a):
@@ -378,7 +378,7 @@
         return a >= count // 2
 
     def give(p):
-        lines = pl.ds(p * units // outer, units // outer)
+        lines = pl.ds(p * units // (2 * outer), units // (2 * outer))
         target = down.at[y, lines]
         return remote(down_hbm.at[0, lines], target, give_s.at[0], give_r.at[0], along)
 
@@ -397,8 +397,8 @@
         def _(a=a):
             cross(0, a).start()
 
-    for p in range(outer):
-        pl.when(deep if p < outer - 1 else final_plane)(lambda: give(p).start())
+    for p in range(2 * outer):
+        pl.when(deep if p < 2 * outer - 1 else final_plane)(lambda: give(p).start())
 
     head_lane = lax.broadcasted_iota(jnp.int32, (rows, narrow), 1) // HN
 
@@ -482,12 +482,11 @@
     def relay(t):
         @pl.when(o >= t)
         def _():
-            for p in range(count // 2):
-                arrived(twin(p), lift_r.at[t - 1, p])
-                for a in (2 * p, 2 * p + 1):
-                    if t < outer - 1:
-                        pl.when(o + 1 < outer)(lambda: lift(t, a).start())
-                    pl.when(crosses(t, a))(lambda: cross(t, a).start())
+            for a in range(count):
+                arrived(blocks[a].at[0], lift_r.at[t - 1, a])
+                if t < outer - 1:
+                    pl.when(o + 1 < outer)(lambda: lift(t, a).start())
+                pl.when(crosses(t, a))(lambda: cross(t, a).start())
 
     def own(t):
         @pl.when(o >= t)
@@ -764,44 +763,76 @@
     loads[0].wait()
     loads[1].wait()
     settle()
-    pl.when(o == outer - 2)(lambda: give(outer - 1).start())
     project()
     ready()
     dispatch()
     for copy in loads[2:]:
         copy.wait()
 
-    @pl.when(deep)
+    @pl.when(final_plane)
     def _():
         begin(0)
+        begin(3)
+        pass_on(0)
         begin(1)
-        pass_on(0)
         begin(2)
-        begin(3)
-        pass_on(1)
+        pass_on(3)
         corner(0)
         enter(0)
         complete()
+        pass_on(1)
+        corner(3)
+        mix(0)
+        enter(3)
         pass_on(2)
+        pair(0)
         corner(1)
-        mix(0)
         enter(1)
-        pass_on(3)
-        pair(0)
+        mix(3)
+        pair(3)
+        corner(2)
+        mix(1)
+        enter(2)
+        leave(0)
+        pair(1)
+        mix(2)
+        leave(3)
+        pair(2)
+        leave(1)
+        leave(2)
+
+    @pl.when(o == outer - 2)
+    def _():
+        begin(2)
+        begin(0)
+        pass_on(2)
+        pass_on(0)
+        give(2 * outer - 1).start()
         corner(2)
         enter(2)
+        begin(3)
+        begin(1)
+        complete()
+        pass_on(3)
+        corner(0)
+        mix(2)
+        enter(0)
+        pass_on(1)
+        pair(2)
+        corner(3)
+        enter(3)
+        mix(0)
+        pair(0)
+        corner(1)
+        mix(3)
+        enter(1)
+        leave(2)
+        pair(3)
         mix(1)
+        leave(0)
         pair(1)
-        corner(3)
-        mix(2)
-        enter(3)
-        leave(0)
-        pair(2)
-        mix(3)
+        leave(3)
         leave(1)
-        pair(3)
-        leave(2)
-        leave(3)
 
     @pl.when(jnp.logical_not(deep))
     def _():
@@ -817,19 +848,20 @@
         begin(2)
         corner(1)
         feed(1)
+        pl.when(o == outer - 3)(lambda: begin(3))
         pass_on(2)
         turn(0)
         gather(1)
-        begin(3)
-        home(0)
         corner(2)
         feed(2)
+        pl.when(o == outer - 4)(lambda: begin(3))
         pass_on(3)
+        home(0)
         turn(1)
         gather(2)
-        home(1)
         corner(3)
         feed(3)
+        home(1)
         turn(2)
         gather(3)
         home(2)
@@ -989,7 +1021,7 @@
         vmem(tiles, own_rows, features // tiles),
         DMA((5 + tiles,)),
         DMA((outer - 1, 2)),
-        DMA((outer - 1, 2)),
+        DMA((outer - 1, 4)),
         DMA((outer, 2)),
         DMA((outer, 2)),
         DMA((1,)),

time: 79.1 us -> 77.5 us (0.980)
  Pallas kernels: 76.1 us -> 75 us
    pallas_call x1, Pallas kernels: 76.1 us -> 75 us  [fast_body(): pl.pallas_call(functools.partial(layer_kernel, outer, inner, ys), out_sha...]
where the time goes in v5:
time: 77.5 us; the launch traced here: 76.7 us
  Pallas kernels  75 us (97%)
  local copies, waits for them, and re-layouts  1.67 us (2%)
    pallas_call x1, Pallas kernels, fast_body(): pl.pallas_call(functools.partial(layer_kernel, outer, inner, ys), out_sha...  75 us
    unnamed x1, local copies, waits for them, and re-layouts  1.67 us

profile of v5, /device:TPU:16, one launch (start us, length us, event | category | flops | bytes accessed | tf_op | source)
XLA Modules:
  0.0 76.7 jit_solution(10689116135138984822)
XLA Ops:
  0.0 75.0 %shard_map.163 = bf16[64,2048]{1,0:T(8,128)(2,1)} custom-call(f32[1,256]{1,0:T(1,128)} %bitcast.7, f32[2,256]{1,0:T(2,128)} %bitcast.6, s32[2,64]{1,0:T(2,128)} %bitcast.8, f32[2,64]{1,0:T(2,128)} %bitcast.9, bf16[256,128]{1,0:T(8,128)(2,1)} %refs_4_.1, bf16[256,128]{1,0:T(8,128)(2,1)} %refs_5_.1, bf16[256,128]{1,0:T(8,128)(2,1)} %refs_6_.1, ...), custom_call_target="tpu_custom_call" | custom-call | tf_op jit(solution)/shard_map/pallas_call | solution.py:1039
  75.0 1.7 %copy.19 = bf16[64,2048]{1,0:T(8,128)(2,1)} copy(bf16[64,2048]{1,0:T(8,128)(2,1)} %shard_map.163) | data formatting | bytes 524288

commit v6 on v5

--- a/solution.py
+++ b/solution.py
@@ -345,7 +345,7 @@
 
         @pl.when(place + d < places)
         def _(d=d):
-            remote(run, far.at[place], far_s.at[d], far_r.at[d], (place + d, tp)).start()
+            remote(run, far.at[place], far_s.at[0], far_r.at[0], (place + d, tp)).start()
 
     ins, blocks = (kw, vw, kn, vn), (kws, vws, kns, vns)
     count = len(ins)
@@ -468,9 +468,9 @@
 
     for d in range(1, places):
 
-        @pl.when(place >= d)
+        @pl.when(place == d)
         def _(d=d):
-            arrived(far.at[place - d], far_r.at[d])
+            arrived(far.at[pl.ds(0, d)], far_r.at[0])
 
     def visit(slot):
         offset = jnp.zeros((far.shape[1], 1), jnp.float32)
@@ -826,13 +826,13 @@
         corner(1)
         mix(3)
         enter(1)
-        leave(2)
         pair(3)
+        leave(0)
         mix(1)
-        leave(0)
         pair(1)
         leave(3)
         leave(1)
+        leave(2)
 
     @pl.when(jnp.logical_not(deep))
     def _():
@@ -885,9 +885,10 @@
 
     for d in range(1, places):
 
-        @pl.when(place + d < places)
+        @pl.when(place + d == places - 1)
         def _(d=d):
-            remote(run, far.at[place], far_s.at[d], far_r.at[d], (place + d, tp)).wait_send()
+            sums = far.at[pl.ds(0, d)]
+            remote(sums, sums, far_s.at[0], far_r.at[0], mate).wait_send()
 
     others = att.at[pl.ds(0, parts - 1)]
     remote(others, others, swap_s.at[0], swap_r.at[0], mate).wait_send()
@@ -1026,8 +1027,8 @@
         DMA((outer, 2)),
         DMA((1,)),
         DMA((1,)),
-        DMA((places,)),
-        DMA((places,)),
+        DMA((1,)),
+        DMA((1,)),
         DMA((1,)),
         DMA((1,)),
         DMA((1,)),

time: 77.5 us -> 77 us (level)
  no operation moved by 1% of the time
where the time goes in v6:
time: 77 us; the launch traced here: 76.6 us
  Pallas kernels  74.9 us (97%)
  local copies, waits for them, and re-layouts  1.67 us (2%)
    pallas_call x1, Pallas kernels, fast_body(): pl.pallas_call(functools.partial(layer_kernel, outer, inner, ys), out_sha...  74.9 us
    unnamed x1, local copies, waits for them, and re-layouts  1.67 us

profile of v6, /device:TPU:16, one launch (start us, length us, event | category | flops | bytes accessed | tf_op | source)
XLA Modules:
  0.0 76.6 jit_solution(8155096358307971708)
XLA Ops:
  0.0 74.9 %shard_map.163 = bf16[64,2048]{1,0:T(8,128)(2,1)} custom-call(f32[1,256]{1,0:T(1,128)} %bitcast.7, f32[2,256]{1,0:T(2,128)} %bitcast.6, s32[2,64]{1,0:T(2,128)} %bitcast.8, f32[2,64]{1,0:T(2,128)} %bitcast.9, bf16[256,128]{1,0:T(8,128)(2,1)} %refs_4_.1, bf16[256,128]{1,0:T(8,128)(2,1)} %refs_5_.1, bf16[256,128]{1,0:T(8,128)(2,1)} %refs_6_.1, ...), custom_call_target="tpu_custom_call" | custom-call | tf_op jit(solution)/shard_map/pallas_call | solution.py:1040
  74.9 1.7 %copy.19 = bf16[64,2048]{1,0:T(8,128)(2,1)} copy(bf16[64,2048]{1,0:T(8,128)(2,1)} %shard_map.163) | data formatting | bytes 524288
